TPU v7x, 512 devices: a 4x2x32 block of a 4x8x32 slice. The times are simulated.
512 devices in a mesh: grp: 2 (over y), kv: 32 (over z), tp: 8 (over x, core).
Axes of the slice: x: 4, y: 2, z: 32, core: 2. Of those that a mesh axis runs over, the one named last changes fastest.
The devices are a block of a 4x8x32 slice.
Arguments:
- tokens: bfloat16 [256, 2048], P('grp', ('kv', 'tp')), parts along dimension 0, may hold values from -13 to 13, as said below
- state: float32 [256, 16, 128, 128], P(('grp', 'kv'), 'tp'), parts along dimension 0, may hold values from -0.6 to 0.6
- norm_gain: bfloat16 [2048], P('kv'), may hold values from 0.099609375 to 1.8984375
- w_query: bfloat16 [2048, 2048], P('kv', 'tp'), may hold values from -0.125 to 0.125
- w_key: bfloat16 [2048, 2048], P('kv', 'tp'), may hold values from -0.125 to 0.125
- w_value: bfloat16 [2048, 2048], P('kv', 'tp'), may hold values from -0.125 to 0.125
- w_beta: bfloat16 [2048, 16], replicated, may hold values from -0.125 to 0.125
- w_decay: bfloat16 [2048, 16], replicated, may hold values from -0.125 to 0.125
- a_log: float32 [16], P('tp'), may hold values from -3 to 1
- dt_bias: float32 [16], P('tp'), may hold values from -2 to 1
- head_gain: float32 [128], replicated, may hold values from 0.1 to 1.9
- w_out: bfloat16 [2048, 2048], P('tp', 'kv'), may hold values from -0.125 to 0.125
- mixer_gain: bfloat16 [2048], P('kv'), may hold values from 0.099609375 to 1.8984375
- w_up: bfloat16 [2048, 8192], P('kv', 'tp'), may hold values from -0.125 to 0.125
- w_down: bfloat16 [8192, 2048], P('tp', 'kv'), may hold values from -0.0625 to 0.0625
Outputs:
- mixed: bfloat16 [256, 2048], P('grp', ('kv', 'tp')), parts along dimension 0
- new_state: float32 [256, 16, 128, 128], P(('grp', 'kv'), 'tp'), parts along dimension 0
There are 2 independent parts, one for each index of `grp`. A program takes and returns all parts, laid end to end along the dimension named above; an argument that names none is the same for every part. Nothing has to cross between parts.
Inputs may be any that keep to these rules, and one draw needn't show every extreme that they name: `tokens`: activations of order one.
All inputs are finite; a program needn't handle non-finite values.
Results may differ from a plain program's by a relative error of at most 0.019.
Values may be sent and summed in bfloat16 or wider, within the bound.
No kernel may reach another device: no remote copies, remote signals or barrier semaphores. Data moves between devices by JAX's collectives and lax.ppermute only.
A program may use at most 64 MiB of HBM per device.

v0:
```python
import functools

import jax
import jax.numpy as jnp
from jax import lax
from jax.experimental import pallas as pl
from jax.experimental.pallas import tpu as pltpu
from jax.sharding import Mesh
from jax.sharding import PartitionSpec as P


epsilon = 1e-06
bf16 = jnp.bfloat16
f32 = jnp.float32
KV = ("hi", "mid", "pair")
LO = ("mid", "pair")
NEAR = (*LO, "tp")
NEIGHBOURS = 4


def exchange(x, axis):
    return lax.all_to_all(x, axis, split_axis=0, concat_axis=0, tiled=True)


def from_everyone(x, axis):
    return exchange(jnp.broadcast_to(x, (lax.axis_size(axis), *x.shape)), axis)


def dotted(left, right, left_dim, right_dim):
    dims = (((left_dim,), (right_dim,)), ((), ()))
    return lax.dot_general(left, right, dims, preferred_element_type=f32)


def delta_kernel(arrived, state, a_log, dt_bias, head_gain, normed_all, keyed_out, fresh_out, decay_out, *, width):
    n_kv, seq, _ = arrived.shape
    heads = state.shape[1]
    size = state.shape[3]
    main = 3 * size
    sums = []
    for head in range(heads):
        total = arrived[head].astype(f32)
        for source in range(head + heads, n_kv, heads):
            total = total + arrived[source].astype(f32)
        sums.append(total)
    gates = sums[0][:, main:]
    for total in sums[1:]:
        gates = gates + total[:, main:]
    first = lax.rsqrt(gates[:, 2 * heads : 2 * heads + 1] / width + epsilon)
    normed = []
    for head in range(heads):
        pre = first * sums[head][:, :main]
        query, key, value = (pre[:, n * size : (n + 1) * size] for n in range(3))
        query = query * lax.rsqrt(jnp.sum(query * query, axis=1, keepdims=True) + epsilon)
        key = key * lax.rsqrt(jnp.sum(key * key, axis=1, keepdims=True) + epsilon)
        beta = jax.nn.sigmoid(first * gates[:, head : head + 1])
        logit = first * gates[:, heads + head : heads + head + 1] + dt_bias[:, head : head + 1]
        soft = jnp.maximum(logit, 0.0) + jnp.log1p(jnp.exp(-jnp.abs(logit)))
        decay = jnp.exp(-jnp.exp(a_log[:, head : head + 1]) * soft)
        turned = jnp.transpose(jnp.concatenate([query, key], axis=0))
        reads = []
        for row in range(seq):
            matrix = state[row, head]
            reads.append(
                (
                    jnp.sum(matrix * turned[:, row : row + 1], axis=0, keepdims=True),
                    jnp.sum(matrix * turned[:, seq + row : seq + row + 1], axis=0, keepdims=True),
                )
            )
        query_read = jnp.concatenate([r[0] for r in reads], axis=0)
        key_read = jnp.concatenate([r[1] for r in reads], axis=0)
        fresh = beta * (value - decay * key_read)
        both = jnp.sum(query * key, axis=1, keepdims=True)
        reading = decay * query_read + both * fresh
        square = jnp.sum(reading * reading, axis=1, keepdims=True) / size
        normed.append(reading * lax.rsqrt(square + epsilon) * head_gain[...])
        keyed_out[head] = key
        fresh_out[head] = fresh
        decay_out[head] = jnp.broadcast_to(decay, (seq, size))
    whole = jnp.concatenate(normed, axis=1).astype(bf16)
    for target in range(n_kv):
        normed_all[target] = whole


def state_kernel(state, keyed, fresh, decay, new_state):
    seq, heads, _, _ = state.shape
    for head in range(heads):
        turned = jnp.transpose(jnp.concatenate([keyed[head], decay[head]], axis=0))
        for row in range(seq):
            column = turned[:, row : row + 1]
            scale = turned[:, seq + row : seq + row + 1]
            new_state[row, head] = scale * state[row, head] + column * fresh[head, row : row + 1, :]


def delta_update(arrived, state, a_log, dt_bias, head_gain, width):
    n_kv, seq, _ = arrived.shape
    heads, size = state.shape[1:3]
    small = pltpu.VMEM((heads, seq, size), f32)
    arrived = pltpu.with_memory_space_constraint(arrived, pltpu.VMEM)
    state = pltpu.with_memory_space_constraint(state, pltpu.VMEM)
    return pl.pallas_call(
        functools.partial(delta_kernel, width=width),
        out_shape=(pltpu.VMEM((n_kv, seq, heads * size), bf16), small, small, small),
    )(arrived, state, a_log[None], dt_bias[None], head_gain[None])


def state_update(state, keyed, fresh, decay):
    small = [pltpu.with_memory_space_constraint(x, pltpu.VMEM) for x in (keyed, fresh, decay)]
    return pl.pallas_call(state_kernel, out_shape=jax.ShapeDtypeStruct(state.shape, f32))(state, *small)


def mixer_weights(w_up, w_down, mixer_gain):
    near = lax.axis_size(LO)
    me = lax.axis_index(LO)
    block, wide = w_up.shape
    share = wide // near
    gained = (w_up.astype(f32) * mixer_gain.astype(f32)[:, None]).astype(bf16)
    both = jnp.concatenate([gained, w_down.T], axis=0)
    both = both.reshape(2 * block, near, share).transpose(1, 0, 2)
    whole = jnp.zeros_like(both)
    for step in range(near):
        piece = lax.dynamic_slice_in_dim(both, me ^ step, 1, axis=0)
        if step:
            piece = lax.ppermute(piece, LO, [(i, i ^ step) for i in range(near)])
        whole = lax.dynamic_update_slice_in_dim(whole, piece, me ^ step, axis=0)
    up = whole[:, :block].reshape(near * block, share)
    down_t = whole[:, block:].reshape(near * block, share)
    return up, down_t


def local(
    tokens,
    state,
    norm_gain,
    w_query,
    w_key,
    w_value,
    w_beta,
    w_decay,
    a_log,
    dt_bias,
    head_gain,
    w_out,
    mixer_gain,
    w_up,
    w_down,
):
    seq_here, heads_here, head_size = state.shape[:3]
    n_kv = lax.axis_size(KV)
    n_tp = lax.axis_size("tp")
    n_near = lax.axis_size(LO)
    width = w_beta.shape[0]
    rows, own = tokens.shape
    block = own * n_tp
    kv_index = lax.axis_index(KV)
    tp_index = lax.axis_index("tp")
    side = lax.axis_index("pair")
    columns = heads_here * head_size
    assert heads_here == lax.axis_size("pair")

    tokens_t = tokens.T
    gain = norm_gain.astype(f32)[:, None]
    split = lambda w: w.reshape(block, heads_here, head_size).transpose(1, 0, 2)
    by_head = jnp.concatenate([split(w_query), split(w_key), split(w_value)], axis=2)
    by_head = (by_head.astype(f32) * gain).astype(bf16)
    kept = lax.dynamic_index_in_dim(by_head, side, 0, keepdims=False)
    given = lax.dynamic_index_in_dim(by_head, 1 - side, 0, keepdims=False)
    taken = lax.ppermute(given, "pair", [(0, 1), (1, 0)])

    both = from_everyone(tokens_t, ("pair", "tp")).reshape(2, block, rows)
    mine = lax.dynamic_index_in_dim(both, side, 0, keepdims=False)
    other = lax.dynamic_index_in_dim(both, 1 - side, 0, keepdims=False)
    inputs = mine.astype(f32)
    scaled = (inputs * gain).astype(bf16)
    squares = jnp.sum(inputs * inputs, axis=0)
    at = (kv_index * block, tp_index * heads_here)
    beta_rows = lax.dynamic_slice(w_beta, at, (block, heads_here))
    decay_rows = lax.dynamic_slice(w_decay, at, (block, heads_here))
    parts = [
        (dotted(mine, kept, 0, 0) + dotted(other, taken, 0, 0)).astype(bf16),
        dotted(scaled, jnp.concatenate([beta_rows, decay_rows], axis=1), 0, 0).astype(bf16),
        squares[:, None].astype(bf16),
    ]
    sent = jnp.concatenate(parts, axis=1).reshape(n_kv, seq_here, -1)
    arrived = exchange(sent, KV)
    up, down_t = mixer_weights(w_up, w_down, mixer_gain)
    normed_all, keyed, fresh, decay = delta_update(arrived, state, a_log, dt_bias, head_gain, width)
    every = exchange(normed_all, KV).reshape(rows, columns)
    new_state = state_update(state, keyed, fresh, decay)
    head_part = dotted(w_out, every, 0, 1).astype(bf16)
    attended = from_everyone(head_part, "tp").astype(f32).sum(axis=0)
    middle_block = (inputs + attended).astype(bf16)
    middle_own = lax.dynamic_slice_in_dim(middle_block, tp_index * own, own, axis=0)

    middle = from_everyone(middle_block, LO).reshape(n_near * block, rows)
    middle_f = middle.astype(f32)
    squares_two = jnp.sum(middle_f * middle_f, axis=0, keepdims=True)
    hidden_part = dotted(up, middle, 0, 0)
    far = lax.axis_size("hi")
    hidden_part = hidden_part.reshape(far, -1, rows)
    tail = jnp.broadcast_to(squares_two, (far, 8, rows))
    sent = jnp.concatenate([hidden_part, tail], axis=1).astype(bf16)
    sums = exchange(sent, "hi").astype(f32).sum(axis=0)
    second = lax.rsqrt(sums[-1:] / width + epsilon)
    hidden_own = jnp.square(jax.nn.relu(second * sums[:-8])).astype(bf16)
    hidden = from_everyone(hidden_own, "hi").reshape(-1, rows)
    down_part = dotted(down_t, hidden, 1, 0).astype(bf16)
    arrived = exchange(down_part.reshape(n_near * n_tp, own, rows), NEAR)
    lowered = arrived.astype(f32).sum(axis=0)
    mixed = (middle_own.astype(f32) + lowered).astype(bf16).T
    return (mixed, new_state)


def solution(mesh):
    near = min(NEIGHBOURS, mesh.shape["kv"])
    devices = mesh.devices.reshape(mesh.shape["grp"], -1, near // 2, 2, mesh.shape["tp"])
    fine = Mesh(devices, ("grp", *KV, "tp"))
    every = (*KV, "tp")
    return jax.shard_map(
        local,
        mesh=fine,
        in_specs=(
            P("grp", every),
            P(("grp", *KV), "tp", None, None),
            P(KV),
            P(KV, "tp"),
            P(KV, "tp"),
            P(KV, "tp"),
            P(),
            P(),
            P("tp"),
            P("tp"),
            P(),
            P("tp", KV),
            P(KV),
            P(KV, "tp"),
            P("tp", KV),
        ),
        out_specs=(P("grp", every), P(("grp", *KV), "tp", None, None)),
        check_vma=False,
    )
```

profile of v0, /device:TPU:33, one launch (start us, length us, event | category | flops | bytes accessed | tf_op | source)
XLA Modules:
  0.0 221.1 jit_solution(9075665370152406865)
XLA Ops:
  0.6 0.0 copy-start
  0.6 1.3 broadcast_in_dim.33
  2.0 0.0 copy-start.4
  2.0 44.9 %all-to-all-start = ((bf16[16,8,128]{2,1,0:T(8,128)(2,1)}), bf16[16,8,128]{2,1,0:T(8,128)(2,1)S(1)}, u32[]{:S(2)}, u32[]{:S(2)}) async-start(bf16[16,8,128]{2,1,0:T(8,128)(2,1)} %broadcast_in_dim.33), calls=%async_computation | async-start | bytes 65536 | tf_op jit(solution)/shard_map/all_to_all | solution.py:22
  46.8 0.0 copy-start.7
  46.8 0.6 copy-done.7
  47.5 0.0 copy-done.4
  47.5 0.0 copy-start.5
  47.5 0.7 copy-done.5
  48.2 0.0 copy-start.6
  48.3 0.7 copy-done.6
  49.0 0.1 multiply_convert_fusion.1
  49.2 0.2 constant_dynamic-slice_fusion.5
  49.4 3.4 %collective-permute-start = (bf16[64,384]{1,0:T(8,128)(2,1)S(1)}, bf16[64,384]{1,0:T(8,128)(2,1)S(1)}, u32[]{:S(2)}, u32[]{:S(2)}) collective-permute-start(bf16[64,384]{1,0:T(8,128)(2,1)S(1)} %bitcast.77), channel_id=1, source_target_pairs={{0,8},{8,0},{1,9},{9,1},{2,10},{10,2},{3,11},{11,3},{4,12},{12,4},... | collective-permute-start | bytes 147464 | tf_op jit(solution)/shard_map/ppermute | solution.py:167
  52.9 0.8 dynamic_slice.40
  53.6 0.8 dynamic_slice.39
  54.4 0.0 all-to-all-done
  54.4 0.2 fusion.3
  54.6 0.2 convolution_convert_fusion.3
  54.8 0.2 convert_element_type.103
  55.1 0.1 copy.40
  55.2 0.0 copy-start.1
  55.2 0.0 collective-permute-done
  55.2 0.2 fusion
  55.5 0.1 pad_maximum_fusion.1
  55.6 36.0 %all_to_all.40.arrived = bf16[32,4,389]{2,1,0:T(4,128)(2,1)S(1)} all-to-all(bf16[32,4,389]{2,1,0:T(4,128)(2,1)S(1)} %pad_maximum_fusion.1), channel_id=1, replica_groups=mesh['grp'=2,'hi'=8,'mid'=2,'pair'=2,'tp'=8] {'hi','mid','pair'}, dimensions={0} | all-to-all | bytes 199168 | tf_op jit(solution)/shard_map/all_to_all | solution.py:22
  91.6 0.0 copy-done.1
  91.6 2.2 %shard_map.158 = (bf16[32,4,256]{2,1,0:T(4,128)(2,1)}, f32[2,4,128]{2,1,0:T(4,128)S(1)}, f32[2,4,128]{2,1,0:T(4,128)S(1)}, f32[2,4,128]{2,1,0:T(4,128)S(1)}) custom-call(bf16[32,4,389]{2,1,0:T(4,128)(2,1)S(1)} %all_to_all.40.arrived, f32[4,2,128,128]{3,2,1,0:T(8,128)S(1)} %copy-done.1, f32[1,2]{1,0:T(1,128)} %bitcast.79, f32[1,2]{1,0:T(1,128)} %bitcast.80, ...), custom_call_target="tpu_custom_call" | custom-call | tf_op jit(solution)/shard_map/pallas_call | solution.py:100
  93.8 5.0 %all-to-all-start.2 = ((bf16[32,4,256]{2,1,0:T(4,128)(2,1)}), bf16[32,4,256]{2,1,0:T(4,128)(2,1)S(1)}, u32[]{:S(2)}, u32[]{:S(2)}) async-start(bf16[32,4,256]{2,1,0:T(4,128)(2,1)} %get-tuple-element.6), calls=%async_computation.2 | async-start | bytes 131072 | tf_op jit(solution)/shard_map/all_to_all | solution.py:22
  98.8 0.0 copy-start.8
  98.8 0.6 copy-done.8
  99.5 0.0 copy-done.2
  99.5 0.1 multiply_convert_fusion
  99.6 0.8 copy-done.3
  100.4 0.2 copy.42
  100.6 0.1 copy.44
  100.7 2.7 %collective-permute-start.1 = (bf16[1,128,256]{2,1,0:T(8,128)(2,1)S(1)}, bf16[1,128,256]{2,1,0:T(8,128)(2,1)S(1)}, u32[]{:S(2)}, u32[]{:S(2)}) collective-permute-start(bf16[1,128,256]{2,1,0:T(8,128)(2,1)S(1)} %bitcast.76), channel_id=1, source_target_pairs={{0,8},{8,0},{16,24},{24,16},{1,9},{9,1},{17,25},{25,17},{2,10},{10... | collective-permute-start | bytes 196616 | tf_op jit(solution)/shard_map/ppermute | solution.py:123
  103.4 0.1 copy.45
  103.6 4.0 %collective-permute-start.2 = (bf16[1,128,256]{2,1,0:T(8,128)(2,1)S(1)}, bf16[1,128,256]{2,1,0:T(8,128)(2,1)S(1)}, u32[]{:S(2)}, u32[]{:S(2)}) collective-permute-start(bf16[1,128,256]{2,1,0:T(8,128)(2,1)S(1)} %bitcast.75), channel_id=1, source_target_pairs={{0,16},{8,24},{16,0},{24,8},{1,17},{9,25},{17,1},{25,9},{2,18},{10... | collective-permute-start | bytes 196616 | tf_op jit(solution)/shard_map/ppermute | solution.py:123
  107.6 0.1 copy.46
  107.7 2.6 %collective-permute-start.3 = (bf16[1,128,256]{2,1,0:T(8,128)(2,1)S(1)}, bf16[1,128,256]{2,1,0:T(8,128)(2,1)S(1)}, u32[]{:S(2)}, u32[]{:S(2)}) collective-permute-start(bf16[1,128,256]{2,1,0:T(8,128)(2,1)S(1)} %bitcast.74), channel_id=1, source_target_pairs={{0,24},{8,16},{16,8},{24,0},{1,25},{9,17},{17,9},{25,1},{2,26},{10... | collective-permute-start | bytes 196616 | tf_op jit(solution)/shard_map/ppermute | solution.py:123
  110.3 0.1 copy.43
  110.5 11.1 %all-to-all-done.2 = bf16[32,4,256]{2,1,0:T(4,128)(2,1)S(1)} async-done(((bf16[32,4,256]{2,1,0:T(4,128)(2,1)}), bf16[32,4,256]{2,1,0:T(4,128)(2,1)S(1)}, u32[]{:S(2)}, u32[]{:S(2)}) %all-to-all-start.2) | async-done | bytes 65568 | tf_op jit(solution)/shard_map/all_to_all | solution.py:22
  121.6 0.0 copy-done
  121.6 0.1 fusion.2
  121.7 0.7 broadcast_in_dim.37
  122.4 8.4 %all-to-all-start.3 = ((bf16[8,64,128]{2,1,0:T(8,128)(2,1)}), bf16[8,64,128]{2,1,0:T(8,128)(2,1)S(1)}, u32[]{:S(2)}, u32[]{:S(2)}) async-start(bf16[8,64,128]{2,1,0:T(8,128)(2,1)} %broadcast_in_dim.37), calls=%async_computation.3 | async-start | bytes 262144 | tf_op jit(solution)/shard_map/all_to_all | solution.py:22
  130.8 0.0 collective-permute-done.1
  130.9 5.2 %all-to-all-done.3 = bf16[8,64,128]{2,1,0:T(8,128)(2,1)S(1)} async-done(((bf16[8,64,128]{2,1,0:T(8,128)(2,1)}), bf16[8,64,128]{2,1,0:T(8,128)(2,1)S(1)}, u32[]{:S(2)}, u32[]{:S(2)}) %all-to-all-start.3) | async-done | bytes 131104 | tf_op jit(solution)/shard_map/all_to_all | solution.py:22
  136.1 0.6 broadcast_in_dim.39
  136.7 3.4 %all-to-all-start.4 = ((bf16[4,64,128]{2,1,0:T(8,128)(2,1)}), bf16[4,64,128]{2,1,0:T(8,128)(2,1)S(1)}, u32[]{:S(2)}, u32[]{:S(2)}) async-start(bf16[4,64,128]{2,1,0:T(8,128)(2,1)} %broadcast_in_dim.39), calls=%async_computation.4 | async-start | bytes 131072 | tf_op jit(solution)/shard_map/all_to_all | solution.py:22
  140.1 0.0 collective-permute-done.2
  140.1 0.0 collective-permute-done.3
  140.2 0.1 copy.47
  140.3 4.3 %all-to-all-done.4 = bf16[4,64,128]{2,1,0:T(8,128)(2,1)S(1)} async-done(((bf16[4,64,128]{2,1,0:T(8,128)(2,1)}), bf16[4,64,128]{2,1,0:T(8,128)(2,1)S(1)}, u32[]{:S(2)}, u32[]{:S(2)}) %all-to-all-start.4) | async-done | bytes 65568 | tf_op jit(solution)/shard_map/all_to_all | solution.py:22
  144.6 0.2 convolution_convert_fusion.1
  144.8 0.1 multiply_reduce_fusion
  144.9 32.2 %all_to_all.41 = bf16[8,40,128]{2,1,0:T(8,128)(2,1)S(1)} all-to-all(bf16[8,40,128]{2,1,0:T(8,128)(2,1)S(1)} %pad_maximum_fusion.2), channel_id=1, replica_groups=mesh['grp'=2,'hi'=8,'mid'=2,'pair'=2,'tp'=8] {'hi'}, dimensions={0} | all-to-all | bytes 163840 | tf_op jit(solution)/shard_map/all_to_all | solution.py:22
  177.2 25.9 %all_to_all.42 = bf16[8,32,128]{2,1,0:T(8,128)(2,1)S(1)} all-to-all(bf16[8,32,128]{2,1,0:T(8,128)(2,1)S(1)} %broadcast_in_dim.41), channel_id=1, replica_groups=mesh['grp'=2,'hi'=8,'mid'=2,'pair'=2,'tp'=8] {'hi'}, dimensions={0} | all-to-all | bytes 131072 | tf_op jit(solution)/shard_map/all_to_all | solution.py:22
  203.0 0.8 fusion.1
  203.8 9.0 %all-to-all-start.7 = ((bf16[32,8,128]{2,1,0:T(8,128)(2,1)}), bf16[32,8,128]{2,1,0:T(8,128)(2,1)S(1)}, u32[]{:S(2)}, u32[]{:S(2)}) async-start(bf16[32,8,128]{2,1,0:T(8,128)(2,1)} %fusion.1), calls=%async_computation.7 | async-start | bytes 131072 | tf_op jit(solution)/shard_map/all_to_all | solution.py:22
  212.8 2.3 %shard_map.159 = f32[4,2,128,128]{3,2,1,0:T(8,128)} custom-call(f32[4,2,128,128]{3,2,1,0:T(8,128)} %state.3, f32[2,4,128]{2,1,0:T(4,128)S(1)} %get-tuple-element.7.keyed, f32[2,4,128]{2,1,0:T(4,128)S(1)} %get-tuple-element.8.fresh, f32[2,4,128]{2,1,0:T(4,128)S(1)} %get-tuple-element.9.decay), custom_call_target="tpu_custom_call" | custom-call | tf_op jit(solution)/shard_map/pallas_call | solution.py:108
  215.1 5.4 %all-to-all-done.7 = bf16[32,8,128]{2,1,0:T(8,128)(2,1)S(1)} async-done(((bf16[32,8,128]{2,1,0:T(8,128)(2,1)}), bf16[32,8,128]{2,1,0:T(8,128)(2,1)S(1)}, u32[]{:S(2)}, u32[]{:S(2)}) %all-to-all-start.7) | async-done | bytes 65568 | tf_op jit(solution)/shard_map/all_to_all | solution.py:22
  220.5 0.6 fusion.23
  (28 shorter events, 0.4 us)
Async XLA Ops:
  0.6 120.9 %copy-start = (bf16[256,64]{0,1:T(8,128)(2,1)S(1)}, bf16[256,64]{0,1:T(8,128)(2,1)}, u32[]{:S(2)}) copy-start(bf16[256,64]{0,1:T(8,128)(2,1)} %param.26) | copy-start | bytes 98308
  2.0 45.5 %copy-start.4 = (bf16[64,256]{1,0:T(8,128)(2,1)S(1)}, bf16[64,256]{1,0:T(8,128)(2,1)}, u32[]{:S(2)}) copy-start(bf16[64,256]{1,0:T(8,128)(2,1)} %param.20) | copy-start | bytes 98308
  2.0 52.4 %all-to-all-start = ((bf16[16,8,128]{2,1,0:T(8,128)(2,1)}), bf16[16,8,128]{2,1,0:T(8,128)(2,1)S(1)}, u32[]{:S(2)}, u32[]{:S(2)}) async-start(bf16[16,8,128]{2,1,0:T(8,128)(2,1)} %broadcast_in_dim.33), calls=%async_computation | async-start | bytes 65536 | tf_op jit(solution)/shard_map/all_to_all | solution.py:22
  46.8 0.7 copy-start.7
  47.5 0.8 copy-start.5
  48.2 0.8 copy-start.6
  49.4 5.8 %collective-permute-start = (bf16[64,384]{1,0:T(8,128)(2,1)S(1)}, bf16[64,384]{1,0:T(8,128)(2,1)S(1)}, u32[]{:S(2)}, u32[]{:S(2)}) collective-permute-start(bf16[64,384]{1,0:T(8,128)(2,1)S(1)} %bitcast.77), channel_id=1, source_target_pairs={{0,8},{8,0},{1,9},{9,1},{2,10},{10,2},{3,11},{11,3},{4,12},{12,4},... | collective-permute-start | bytes 147464 | tf_op jit(solution)/shard_map/ppermute | solution.py:167
  55.2 36.4 %copy-start.1 = (f32[4,2,128,128]{3,2,1,0:T(8,128)S(1)}, f32[4,2,128,128]{3,2,1,0:T(8,128)}, u32[]{:S(2)}) copy-start(f32[4,2,128,128]{3,2,1,0:T(8,128)} %state.3) | copy-start | bytes 1572868
  93.8 5.7 %copy-start.2 = (bf16[64,1024]{1,0:T(8,128)(2,1)S(1)}, bf16[64,1024]{1,0:T(8,128)(2,1)}, u32[]{:S(2)}) copy-start(bf16[64,1024]{1,0:T(8,128)(2,1)} %param.28) | copy-start | bytes 393220
  93.8 27.7 %all-to-all-start.2 = ((bf16[32,4,256]{2,1,0:T(4,128)(2,1)}), bf16[32,4,256]{2,1,0:T(4,128)(2,1)S(1)}, u32[]{:S(2)}, u32[]{:S(2)}) async-start(bf16[32,4,256]{2,1,0:T(4,128)(2,1)} %get-tuple-element.6), calls=%async_computation.2 | async-start | bytes 131072 | tf_op jit(solution)/shard_map/all_to_all | solution.py:22
  98.8 0.7 copy-start.8
  99.5 0.9 copy-start.3
  100.7 30.1 %collective-permute-start.1 = (bf16[1,128,256]{2,1,0:T(8,128)(2,1)S(1)}, bf16[1,128,256]{2,1,0:T(8,128)(2,1)S(1)}, u32[]{:S(2)}, u32[]{:S(2)}) collective-permute-start(bf16[1,128,256]{2,1,0:T(8,128)(2,1)S(1)} %bitcast.76), channel_id=1, source_target_pairs={{0,8},{8,0},{16,24},{24,16},{1,9},{9,1},{17,25},{25,17},{2,10},{10... | collective-permute-start | bytes 196616 | tf_op jit(solution)/shard_map/ppermute | solution.py:123
  103.6 36.6 %collective-permute-start.2 = (bf16[1,128,256]{2,1,0:T(8,128)(2,1)S(1)}, bf16[1,128,256]{2,1,0:T(8,128)(2,1)S(1)}, u32[]{:S(2)}, u32[]{:S(2)}) collective-permute-start(bf16[1,128,256]{2,1,0:T(8,128)(2,1)S(1)} %bitcast.75), channel_id=1, source_target_pairs={{0,16},{8,24},{16,0},{24,8},{1,17},{9,25},{17,1},{25,9},{2,18},{10... | collective-permute-start | bytes 196616 | tf_op jit(solution)/shard_map/ppermute | solution.py:123
  107.7 32.4 %collective-permute-start.3 = (bf16[1,128,256]{2,1,0:T(8,128)(2,1)S(1)}, bf16[1,128,256]{2,1,0:T(8,128)(2,1)S(1)}, u32[]{:S(2)}, u32[]{:S(2)}) collective-permute-start(bf16[1,128,256]{2,1,0:T(8,128)(2,1)S(1)} %bitcast.74), channel_id=1, source_target_pairs={{0,24},{8,16},{16,8},{24,0},{1,25},{9,17},{17,9},{25,1},{2,26},{10... | collective-permute-start | bytes 196616 | tf_op jit(solution)/shard_map/ppermute | solution.py:123
  122.4 13.6 %all-to-all-start.3 = ((bf16[8,64,128]{2,1,0:T(8,128)(2,1)}), bf16[8,64,128]{2,1,0:T(8,128)(2,1)S(1)}, u32[]{:S(2)}, u32[]{:S(2)}) async-start(bf16[8,64,128]{2,1,0:T(8,128)(2,1)} %broadcast_in_dim.37), calls=%async_computation.3 | async-start | bytes 262144 | tf_op jit(solution)/shard_map/all_to_all | solution.py:22
  136.7 7.9 %all-to-all-start.4 = ((bf16[4,64,128]{2,1,0:T(8,128)(2,1)}), bf16[4,64,128]{2,1,0:T(8,128)(2,1)S(1)}, u32[]{:S(2)}, u32[]{:S(2)}) async-start(bf16[4,64,128]{2,1,0:T(8,128)(2,1)} %broadcast_in_dim.39), calls=%async_computation.4 | async-start | bytes 131072 | tf_op jit(solution)/shard_map/all_to_all | solution.py:22
  203.8 16.6 %all-to-all-start.7 = ((bf16[32,8,128]{2,1,0:T(8,128)(2,1)}), bf16[32,8,128]{2,1,0:T(8,128)(2,1)S(1)}, u32[]{:S(2)}, u32[]{:S(2)}) async-start(bf16[32,8,128]{2,1,0:T(8,128)(2,1)} %fusion.1), calls=%async_computation.7 | async-start | bytes 131072 | tf_op jit(solution)/shard_map/all_to_all | solution.py:22
where the time goes:
time: 222 us; the launch traced here: 221 us
  blocking collectives  94.1 us (42%)
  starting transfers between devices  83.4 us (38%)
  waiting for transfers between devices  25.9 us (12%)
  local copies, waits for them, and re-layouts  9.3 us (4%)
  Pallas kernels  4.49 us (2%)
    all_to_all x3, blocking collectives, exchange(): return lax.all_to_all(x, axis, split_axis=0, concat_axis=0, tiled=True)  94.1 us
    all_to_all x5, starting transfers between devices, exchange(): return lax.all_to_all(x, axis, split_axis=0, concat_axis=0, tiled=True)  70.6 us
    all_to_all x5, waiting for transfers between devices, exchange(): return lax.all_to_all(x, axis, split_axis=0, concat_axis=0, tiled=True)  25.9 us
    ppermute x3, starting transfers between devices, mixer_weights(): piece = lax.ppermute(piece, LO, [(i, i ^ step) for i in range(near)])  9.36 us
  transfers between devices with their start and end apart: 9, of which 4 were waited for; matrix products, arithmetic and copies ran while one was open for 2% of the time, Pallas kernels for 1%

commit v1 on v0

--- a/solution.py
+++ b/solution.py
@@ -31,7 +31,7 @@
     return lax.dot_general(left, right, dims, preferred_element_type=f32)
 
 
-def delta_kernel(arrived, state, a_log, dt_bias, head_gain, normed_all, keyed_out, fresh_out, decay_out, *, width):
+def delta_kernel(arrived, state, a_log, dt_bias, head_gain, normed_all, keyed_out, fresh_out, decay_out, *, width, all_heads):
     n_kv, seq, _ = arrived.shape
     heads = state.shape[1]
     size = state.shape[3]
@@ -45,15 +45,18 @@
     gates = sums[0][:, main:]
     for total in sums[1:]:
         gates = gates + total[:, main:]
-    first = lax.rsqrt(gates[:, 2 * heads : 2 * heads + 1] / width + epsilon)
+    tp_index = lax.axis_index("tp")
+    lane = lax.broadcasted_iota(jnp.int32, gates.shape, 1)
+    at = lambda n: jnp.sum(jnp.where(lane == n, gates, 0.0), axis=1, keepdims=True)
+    first = lax.rsqrt(at(2 * all_heads) / width + epsilon)
     normed = []
     for head in range(heads):
         pre = first * sums[head][:, :main]
         query, key, value = (pre[:, n * size : (n + 1) * size] for n in range(3))
         query = query * lax.rsqrt(jnp.sum(query * query, axis=1, keepdims=True) + epsilon)
         key = key * lax.rsqrt(jnp.sum(key * key, axis=1, keepdims=True) + epsilon)
-        beta = jax.nn.sigmoid(first * gates[:, head : head + 1])
-        logit = first * gates[:, heads + head : heads + head + 1] + dt_bias[:, head : head + 1]
+        beta = jax.nn.sigmoid(first * at(heads * tp_index + head))
+        logit = first * at(all_heads + heads * tp_index + head) + dt_bias[:, head : head + 1]
         soft = jnp.maximum(logit, 0.0) + jnp.log1p(jnp.exp(-jnp.abs(logit)))
         decay = jnp.exp(-jnp.exp(a_log[:, head : head + 1]) * soft)
         turned = jnp.transpose(jnp.concatenate([query, key], axis=0))
@@ -91,16 +94,90 @@
             new_state[row, head] = scale * state[row, head] + column * fresh[head, row : row + 1, :]
 
 
-def delta_update(arrived, state, a_log, dt_bias, head_gain, width):
+def delta_update(arrived, state, a_log, dt_bias, head_gain, width, all_heads):
     n_kv, seq, _ = arrived.shape
     heads, size = state.shape[1:3]
     small = pltpu.VMEM((heads, seq, size), f32)
     arrived = pltpu.with_memory_space_constraint(arrived, pltpu.VMEM)
     state = pltpu.with_memory_space_constraint(state, pltpu.VMEM)
+    whole = pl.BlockSpec(memory_space=pltpu.VMEM)
     return pl.pallas_call(
-        functools.partial(delta_kernel, width=width),
+        functools.partial(delta_kernel, width=width, all_heads=all_heads),
+        in_specs=[whole] * 5,
         out_shape=(pltpu.VMEM((n_kv, seq, heads * size), bf16), small, small, small),
     )(arrived, state, a_log[None], dt_bias[None], head_gain[None])
+
+
+def weights_kernel(*refs):
+    sources, kept, given, gates, held, arrivals = refs[:6], refs[6], refs[7], refs[8], refs[9:15], refs[15]
+    block = kept.shape[0]
+    size = kept.shape[1] // 3
+    side = lax.axis_index("pair")
+    start = pl.multiple_of(lax.axis_index(KV[:2]) * (2 * block), 2 * block)
+    copies = []
+    for n, (source, target) in enumerate(zip(sources, held)):
+        source = source.at[:, pl.ds(start, 2 * block)] if n >= 4 else source
+        copies.append(pltpu.make_async_copy(source, target, arrivals.at[n]))
+    for copy in copies:
+        copy.start()
+    for copy in copies:
+        copy.wait()
+    query, key, value, gain, beta, decay = held
+    wide = gain[...].astype(f32)
+    column = jnp.transpose(jnp.broadcast_to(wide, (8, block)))[:, :1]
+    heads = []
+    for head in range(2):
+        cut = slice(head * size, (head + 1) * size)
+        heads.append([w[:, cut].astype(f32) * column for w in (query, key, value)])
+    for n in range(3):
+        cut = slice(n * size, (n + 1) * size)
+        kept[:, cut] = jnp.where(side == 0, heads[0][n], heads[1][n]).astype(bf16)
+        given[:, cut] = jnp.where(side == 0, heads[1][n], heads[0][n]).astype(bf16)
+    both = jnp.concatenate([beta[...].astype(f32), decay[...].astype(f32)], axis=0)
+    both = jnp.where(side == 0, both[:, :block], both[:, block:])
+    gates[...] = jnp.transpose(both * wide).astype(bf16)
+
+
+def projection_weights(w_query, w_key, w_value, norm_gain, w_beta, w_decay, size):
+    block = w_query.shape[0]
+    assert 2 * block % 128 == 0
+    sources = (w_query, w_key, w_value, norm_gain[None], w_beta.T, w_decay.T)
+    held = [pltpu.VMEM(x.shape, bf16) for x in sources[:4]]
+    held += [pltpu.VMEM((x.shape[0], 2 * block), bf16) for x in sources[4:]]
+    cut = pltpu.VMEM((block, 3 * size), bf16)
+    return pl.pallas_call(
+        weights_kernel,
+        in_specs=[pl.BlockSpec(memory_space=pl.ANY)] * 6,
+        out_shape=(cut, cut, pltpu.VMEM((block, 2 * w_beta.shape[1]), bf16)),
+        scratch_shapes=[*held, pltpu.SemaphoreType.DMA((6,))],
+    )(*sources)
+
+
+def sums_kernel(both, kept, taken, gates, sent):
+    n_kv, seq, columns = sent.shape
+    side = lax.axis_index("pair")
+    mine = jnp.transpose(both[side].astype(f32))
+    other = jnp.transpose(both[1 - side].astype(f32))
+    squares = jnp.sum(mine * mine, axis=1, keepdims=True)
+    mine = mine.astype(bf16)
+    main = dotted(mine, kept[...], 1, 0) + dotted(other.astype(bf16), taken[...], 1, 0)
+    extra = dotted(mine, gates[...], 1, 0)
+    spare = columns - main.shape[1] - extra.shape[1] - 1
+    tail = jnp.concatenate([extra, squares, jnp.zeros((mine.shape[0], spare), f32)], axis=1)
+    whole = jnp.concatenate([main, tail], axis=1)
+    for target in range(n_kv):
+        sent[target] = whole[target * seq : (target + 1) * seq].astype(bf16)
+
+
+def partial_sums(both, kept, taken, gates, n_kv, seq):
+    whole = pl.BlockSpec(memory_space=pltpu.VMEM)
+    columns = kept.shape[1] + 128
+    near = [pltpu.with_memory_space_constraint(x, pltpu.VMEM) for x in (both, kept, taken, gates)]
+    return pl.pallas_call(
+        sums_kernel,
+        in_specs=[whole] * 4,
+        out_shape=jax.ShapeDtypeStruct((n_kv, seq, columns), bf16),
+    )(*near)
 
 
 def state_update(state, keyed, fresh, decay):
@@ -108,20 +185,26 @@
     return pl.pallas_call(state_kernel, out_shape=jax.ShapeDtypeStruct(state.shape, f32))(state, *small)
 
 
-def mixer_weights(w_up, w_down, mixer_gain):
+def mixer_pieces(w_up, w_down, mixer_gain):
     near = lax.axis_size(LO)
     me = lax.axis_index(LO)
     block, wide = w_up.shape
-    share = wide // near
     gained = (w_up.astype(f32) * mixer_gain.astype(f32)[:, None]).astype(bf16)
     both = jnp.concatenate([gained, w_down.T], axis=0)
-    both = both.reshape(2 * block, near, share).transpose(1, 0, 2)
-    whole = jnp.zeros_like(both)
-    for step in range(near):
-        piece = lax.dynamic_slice_in_dim(both, me ^ step, 1, axis=0)
+    both = both.reshape(2 * block, near, wide // near).transpose(1, 0, 2)
+    return [lax.dynamic_index_in_dim(both, me ^ step, 0, keepdims=False) for step in range(near)]
+
+
+def mixer_weights(pieces):
+    near = lax.axis_size(LO)
+    me = lax.axis_index(LO)
+    both, share = pieces[0].shape
+    whole = jnp.zeros((near, both, share), bf16)
+    for step, piece in enumerate(pieces):
         if step:
             piece = lax.ppermute(piece, LO, [(i, i ^ step) for i in range(near)])
-        whole = lax.dynamic_update_slice_in_dim(whole, piece, me ^ step, axis=0)
+        whole = lax.dynamic_update_slice_in_dim(whole, piece[None], me ^ step, axis=0)
+    block = both // 2
     up = whole[:, :block].reshape(near * block, share)
     down_t = whole[:, block:].reshape(near * block, share)
     return up, down_t
@@ -151,39 +234,24 @@
     width = w_beta.shape[0]
     rows, own = tokens.shape
     block = own * n_tp
-    kv_index = lax.axis_index(KV)
     tp_index = lax.axis_index("tp")
     side = lax.axis_index("pair")
     columns = heads_here * head_size
     assert heads_here == lax.axis_size("pair")
 
     tokens_t = tokens.T
-    gain = norm_gain.astype(f32)[:, None]
-    split = lambda w: w.reshape(block, heads_here, head_size).transpose(1, 0, 2)
-    by_head = jnp.concatenate([split(w_query), split(w_key), split(w_value)], axis=2)
-    by_head = (by_head.astype(f32) * gain).astype(bf16)
-    kept = lax.dynamic_index_in_dim(by_head, side, 0, keepdims=False)
-    given = lax.dynamic_index_in_dim(by_head, 1 - side, 0, keepdims=False)
+    kept, given, gates = projection_weights(
+        w_query, w_key, w_value, norm_gain, w_beta, w_decay, head_size
+    )
     taken = lax.ppermute(given, "pair", [(0, 1), (1, 0)])
 
     both = from_everyone(tokens_t, ("pair", "tp")).reshape(2, block, rows)
-    mine = lax.dynamic_index_in_dim(both, side, 0, keepdims=False)
-    other = lax.dynamic_index_in_dim(both, 1 - side, 0, keepdims=False)
-    inputs = mine.astype(f32)
-    scaled = (inputs * gain).astype(bf16)
-    squares = jnp.sum(inputs * inputs, axis=0)
-    at = (kv_index * block, tp_index * heads_here)
-    beta_rows = lax.dynamic_slice(w_beta, at, (block, heads_here))
-    decay_rows = lax.dynamic_slice(w_decay, at, (block, heads_here))
-    parts = [
-        (dotted(mine, kept, 0, 0) + dotted(other, taken, 0, 0)).astype(bf16),
-        dotted(scaled, jnp.concatenate([beta_rows, decay_rows], axis=1), 0, 0).astype(bf16),
-        squares[:, None].astype(bf16),
-    ]
-    sent = jnp.concatenate(parts, axis=1).reshape(n_kv, seq_here, -1)
+    inputs = lax.dynamic_index_in_dim(both, side, 0, keepdims=False).astype(f32)
+    sent = partial_sums(both, kept, taken, gates, n_kv, seq_here)
+    pieces = mixer_pieces(w_up, w_down, mixer_gain)
     arrived = exchange(sent, KV)
-    up, down_t = mixer_weights(w_up, w_down, mixer_gain)
-    normed_all, keyed, fresh, decay = delta_update(arrived, state, a_log, dt_bias, head_gain, width)
+    up, down_t = mixer_weights(pieces)
+    normed_all, keyed, fresh, decay = delta_update(arrived, state, a_log, dt_bias, head_gain, width, w_beta.shape[1])
     every = exchange(normed_all, KV).reshape(rows, columns)
     new_state = state_update(state, keyed, fresh, decay)
     head_part = dotted(w_out, every, 0, 1).astype(bf16)

time: 222 us -> 219 us (0.986)
  blocking collectives: 94.1 us -> 56.3 us
  waiting for transfers between devices: 25.9 us -> 55.6 us
  starting transfers between devices: 83.4 us -> 91.7 us
  local copies, waits for them, and re-layouts: 9.3 us -> 4.97 us
    all_to_all x3 -> x2, blocking collectives: 94.1 us -> 56.3 us  [exchange(): return lax.all_to_all(x, axis, split_axis=0, concat_axis=0, tiled=True)]
    all_to_all x5 -> x6, waiting for transfers between devices: 25.9 us -> 54.1 us  [exchange(): return lax.all_to_all(x, axis, split_axis=0, concat_axis=0, tiled=True)]
    all_to_all x5 -> x6, starting transfers between devices: 70.6 us -> 78.9 us  [exchange(): return lax.all_to_all(x, axis, split_axis=0, concat_axis=0, tiled=True)]
  transfers between devices with their start and end apart: 9 -> 10, of which waited for: 4 -> 6; matrix products, arithmetic and copies ran while one was open for 2% -> 1% of each run, Pallas kernels for 1% -> 2%
where the time goes in v1:
time: 219 us; the launch traced here: 218 us
  starting transfers between devices  91.7 us (42%)
  blocking collectives  56.3 us (26%)
  waiting for transfers between devices  55.6 us (25%)
  Pallas kernels  6.46 us (3%)
  local copies, waits for them, and re-layouts  4.97 us (2%)
    all_to_all x6, starting transfers between devices, exchange(): return lax.all_to_all(x, axis, split_axis=0, concat_axis=0, tiled=True)  78.9 us
    all_to_all x2, blocking collectives, exchange(): return lax.all_to_all(x, axis, split_axis=0, concat_axis=0, tiled=True)  56.3 us
    all_to_all x6, waiting for transfers between devices, exchange(): return lax.all_to_all(x, axis, split_axis=0, concat_axis=0, tiled=True)  54.1 us
    ppermute x3, starting transfers between devices, mixer_weights(): piece = lax.ppermute(piece, LO, [(i, i ^ step) for i in range(near)])  9.36 us
  transfers between devices with their start and end apart: 10, of which 6 were waited for; matrix products, arithmetic and copies ran while one was open for 1% of the time, Pallas kernels for 2%

profile of v1, /device:TPU:33, one launch (start us, length us, event | category | flops | bytes accessed | tf_op | source)
XLA Modules:
  0.0 217.9 jit_solution(473506012356976513)
XLA Ops:
  0.6 0.0 copy-start
  0.6 1.3 broadcast_in_dim.44
  2.0 44.7 %all-to-all-start = ((bf16[16,8,128]{2,1,0:T(8,128)(2,1)}), bf16[16,8,128]{2,1,0:T(8,128)(2,1)S(1)}, u32[]{:S(2)}, u32[]{:S(2)}) async-start(bf16[16,8,128]{2,1,0:T(8,128)(2,1)} %broadcast_in_dim.44), calls=%async_computation | async-start | bytes 65536 | tf_op jit(solution)/shard_map/all_to_all | solution.py:22
  46.7 1.0 shard_map.158
  47.7 3.4 %collective-permute-start = (bf16[64,384]{1,0:T(8,128)(2,1)S(1)}, bf16[64,384]{1,0:T(8,128)(2,1)S(1)}, u32[]{:S(2)}, u32[]{:S(2)}) collective-permute-start(bf16[64,384]{1,0:T(8,128)(2,1)S(1)} %get-tuple-element.10), channel_id=1, source_target_pairs={{0,8},{8,0},{1,9},{9,1},{2,10},{10,2},{3,11},{11,3},{4,12},{12,4},... | collective-permute-start | bytes 147464 | tf_op jit(solution)/shard_map/ppermute | solution.py:246
  51.2 1.5 collective-permute-done.taken
  52.7 0.0 all-to-all-done
  52.7 0.9 shard_map.159
  53.6 0.0 copy-start.2
  53.6 7.9 %all-to-all-start.1 = ((bf16[32,4,512]{2,1,0:T(4,128)(2,1)}), bf16[32,4,512]{2,1,0:T(4,128)(2,1)S(1)}, u32[]{:S(2)}, u32[]{:S(2)}) async-start(bf16[32,4,512]{2,1,0:T(4,128)(2,1)} %shard_map.159), calls=%async_computation.1 | async-start | bytes 262144 | tf_op jit(solution)/shard_map/all_to_all | solution.py:22
  61.5 0.0 copy-start.4
  61.6 0.6 copy-done.4
  62.2 0.0 copy-done.2
  62.2 0.0 copy-start.3
  62.2 0.1 multiply_convert_fusion
  62.3 0.8 copy-done.3
  63.1 0.0 copy-start.1
  63.1 0.2 copy.32
  63.3 26.3 %all-to-all-done.1.arrived = bf16[32,4,512]{2,1,0:T(4,128)(2,1)S(1)} async-done(((bf16[32,4,512]{2,1,0:T(4,128)(2,1)}), bf16[32,4,512]{2,1,0:T(4,128)(2,1)S(1)}, u32[]{:S(2)}, u32[]{:S(2)}) %all-to-all-start.1) | async-done | bytes 131104 | tf_op jit(solution)/shard_map/all_to_all | solution.py:22
  89.7 0.0 copy-done.1
  89.7 2.2 %shard_map.160 = (bf16[32,4,256]{2,1,0:T(4,128)(2,1)}, f32[2,4,128]{2,1,0:T(4,128)S(1)}, f32[2,4,128]{2,1,0:T(4,128)S(1)}, f32[2,4,128]{2,1,0:T(4,128)S(1)}) custom-call(bf16[32,4,512]{2,1,0:T(4,128)(2,1)S(1)} %all-to-all-done.1.arrived, f32[4,2,128,128]{3,2,1,0:T(8,128)S(1)} %copy-done.1, f32[1,2]{1,0:T(1,128)} %bitcast.63, f32[1,2]{1,0:T(1,128)} %bitcast.64, ...), custom_call_target="tpu_custom_call" | custom-call | tf_op jit(solution)/shard_map/pallas_call | solution.py:104
  91.9 5.3 %all-to-all-start.2 = ((bf16[32,4,256]{2,1,0:T(4,128)(2,1)}), bf16[32,4,256]{2,1,0:T(4,128)(2,1)S(1)}, u32[]{:S(2)}, u32[]{:S(2)}) async-start(bf16[32,4,256]{2,1,0:T(4,128)(2,1)} %get-tuple-element.12), calls=%async_computation.2 | async-start | bytes 131072 | tf_op jit(solution)/shard_map/all_to_all | solution.py:22
  97.2 0.1 copy.34
  97.3 2.7 %collective-permute-start.1 = (bf16[128,256]{1,0:T(8,128)(2,1)S(1)}, bf16[128,256]{1,0:T(8,128)(2,1)S(1)}, u32[]{:S(2)}, u32[]{:S(2)}) collective-permute-start(bf16[128,256]{1,0:T(8,128)(2,1)S(1)} %bitcast.60), channel_id=1, source_target_pairs={{0,8},{8,0},{16,24},{24,16},{1,9},{9,1},{17,25},{25,17},{2,10},{10... | collective-permute-start | bytes 196616 | tf_op jit(solution)/shard_map/ppermute | solution.py:205
  100.0 0.1 copy.35
  100.2 4.0 %collective-permute-start.2 = (bf16[128,256]{1,0:T(8,128)(2,1)S(1)}, bf16[128,256]{1,0:T(8,128)(2,1)S(1)}, u32[]{:S(2)}, u32[]{:S(2)}) collective-permute-start(bf16[128,256]{1,0:T(8,128)(2,1)S(1)} %bitcast.59), channel_id=1, source_target_pairs={{0,16},{8,24},{16,0},{24,8},{1,17},{9,25},{17,1},{25,9},{2,18},{10... | collective-permute-start | bytes 196616 | tf_op jit(solution)/shard_map/ppermute | solution.py:205
  104.2 0.1 copy.36
  104.3 2.6 %collective-permute-start.3 = (bf16[128,256]{1,0:T(8,128)(2,1)S(1)}, bf16[128,256]{1,0:T(8,128)(2,1)S(1)}, u32[]{:S(2)}, u32[]{:S(2)}) collective-permute-start(bf16[128,256]{1,0:T(8,128)(2,1)S(1)} %bitcast.58), channel_id=1, source_target_pairs={{0,24},{8,16},{16,8},{24,0},{1,25},{9,17},{17,9},{25,1},{2,26},{10... | collective-permute-start | bytes 196616 | tf_op jit(solution)/shard_map/ppermute | solution.py:205
  106.9 0.1 copy.33
  107.1 0.0 collective-permute-done.1
  107.1 12.8 %all-to-all-done.2 = bf16[32,4,256]{2,1,0:T(4,128)(2,1)S(1)} async-done(((bf16[32,4,256]{2,1,0:T(4,128)(2,1)}), bf16[32,4,256]{2,1,0:T(4,128)(2,1)S(1)}, u32[]{:S(2)}, u32[]{:S(2)}) %all-to-all-start.2) | async-done | bytes 65568 | tf_op jit(solution)/shard_map/all_to_all | solution.py:22
  120.0 0.0 copy-done
  120.0 0.1 fusion.1
  120.1 0.7 broadcast_in_dim.49
  120.8 8.6 %all-to-all-start.3 = ((bf16[8,64,128]{2,1,0:T(8,128)(2,1)}), bf16[8,64,128]{2,1,0:T(8,128)(2,1)S(1)}, u32[]{:S(2)}, u32[]{:S(2)}) async-start(bf16[8,64,128]{2,1,0:T(8,128)(2,1)} %broadcast_in_dim.49), calls=%async_computation.3 | async-start | bytes 262144 | tf_op jit(solution)/shard_map/all_to_all | solution.py:22
  129.5 0.0 collective-permute-done.2
  129.5 5.2 %all-to-all-done.3 = bf16[8,64,128]{2,1,0:T(8,128)(2,1)S(1)} async-done(((bf16[8,64,128]{2,1,0:T(8,128)(2,1)}), bf16[8,64,128]{2,1,0:T(8,128)(2,1)S(1)}, u32[]{:S(2)}, u32[]{:S(2)}) %all-to-all-start.3) | async-done | bytes 131104 | tf_op jit(solution)/shard_map/all_to_all | solution.py:22
  134.7 0.6 broadcast_in_dim.54
  135.4 3.4 %all-to-all-start.4 = ((bf16[4,64,128]{2,1,0:T(8,128)(2,1)}), bf16[4,64,128]{2,1,0:T(8,128)(2,1)S(1)}, u32[]{:S(2)}, u32[]{:S(2)}) async-start(bf16[4,64,128]{2,1,0:T(8,128)(2,1)} %broadcast_in_dim.54), calls=%async_computation.4 | async-start | bytes 131072 | tf_op jit(solution)/shard_map/all_to_all | solution.py:22
  138.8 0.0 collective-permute-done.3
  138.8 0.1 copy.37
  138.9 4.4 %all-to-all-done.4 = bf16[4,64,128]{2,1,0:T(8,128)(2,1)S(1)} async-done(((bf16[4,64,128]{2,1,0:T(8,128)(2,1)}), bf16[4,64,128]{2,1,0:T(8,128)(2,1)S(1)}, u32[]{:S(2)}, u32[]{:S(2)}) %all-to-all-start.4) | async-done | bytes 65568 | tf_op jit(solution)/shard_map/all_to_all | solution.py:22
  143.3 0.2 convolution_convert_fusion.1
  143.5 0.1 multiply_reduce_fusion
  143.5 30.4 %all_to_all.40 = bf16[8,40,128]{2,1,0:T(8,128)(2,1)S(1)} all-to-all(bf16[8,40,128]{2,1,0:T(8,128)(2,1)S(1)} %pad_maximum_fusion.1), channel_id=1, replica_groups=mesh['grp'=2,'hi'=8,'mid'=2,'pair'=2,'tp'=8] {'hi'}, dimensions={0} | all-to-all | bytes 163840 | tf_op jit(solution)/shard_map/all_to_all | solution.py:22
  174.0 25.9 %all_to_all.41 = bf16[8,32,128]{2,1,0:T(8,128)(2,1)S(1)} all-to-all(bf16[8,32,128]{2,1,0:T(8,128)(2,1)S(1)} %broadcast_in_dim.56), channel_id=1, replica_groups=mesh['grp'=2,'hi'=8,'mid'=2,'pair'=2,'tp'=8] {'hi'}, dimensions={0} | all-to-all | bytes 131072 | tf_op jit(solution)/shard_map/all_to_all | solution.py:22
  199.9 0.8 fusion
  200.7 9.0 %all-to-all-start.7 = ((bf16[32,8,128]{2,1,0:T(8,128)(2,1)}), bf16[32,8,128]{2,1,0:T(8,128)(2,1)S(1)}, u32[]{:S(2)}, u32[]{:S(2)}) async-start(bf16[32,8,128]{2,1,0:T(8,128)(2,1)} %fusion), calls=%async_computation.7 | async-start | bytes 131072 | tf_op jit(solution)/shard_map/all_to_all | solution.py:22
  209.7 2.3 %shard_map.161 = f32[4,2,128,128]{3,2,1,0:T(8,128)} custom-call(f32[4,2,128,128]{3,2,1,0:T(8,128)} %state.3, f32[2,4,128]{2,1,0:T(4,128)S(1)} %get-tuple-element.13.keyed, f32[2,4,128]{2,1,0:T(4,128)S(1)} %get-tuple-element.14.fresh, f32[2,4,128]{2,1,0:T(4,128)S(1)} %get-tuple-element.15.decay), custom_call_target="tpu_custom_call" | custom-call | tf_op jit(solution)/shard_map/pallas_call | solution.py:185
  211.9 5.4 %all-to-all-done.7 = bf16[32,8,128]{2,1,0:T(8,128)(2,1)S(1)} async-done(((bf16[32,8,128]{2,1,0:T(8,128)(2,1)}), bf16[32,8,128]{2,1,0:T(8,128)(2,1)S(1)}, u32[]{:S(2)}, u32[]{:S(2)}) %all-to-all-start.7) | async-done | bytes 65568 | tf_op jit(solution)/shard_map/all_to_all | solution.py:22
  217.3 0.6 fusion.6
  (19 shorter events, 0.3 us)
Async XLA Ops:
  0.6 119.4 %copy-start = (bf16[256,64]{0,1:T(8,128)(2,1)S(1)}, bf16[256,64]{0,1:T(8,128)(2,1)}, u32[]{:S(2)}) copy-start(bf16[256,64]{0,1:T(8,128)(2,1)} %param.26) | copy-start | bytes 98308
  2.0 50.7 %all-to-all-start = ((bf16[16,8,128]{2,1,0:T(8,128)(2,1)}), bf16[16,8,128]{2,1,0:T(8,128)(2,1)S(1)}, u32[]{:S(2)}, u32[]{:S(2)}) async-start(bf16[16,8,128]{2,1,0:T(8,128)(2,1)} %broadcast_in_dim.44), calls=%async_computation | async-start | bytes 65536 | tf_op jit(solution)/shard_map/all_to_all | solution.py:22
  47.7 5.0 %collective-permute-start = (bf16[64,384]{1,0:T(8,128)(2,1)S(1)}, bf16[64,384]{1,0:T(8,128)(2,1)S(1)}, u32[]{:S(2)}, u32[]{:S(2)}) collective-permute-start(bf16[64,384]{1,0:T(8,128)(2,1)S(1)} %get-tuple-element.10), channel_id=1, source_target_pairs={{0,8},{8,0},{1,9},{9,1},{2,10},{10,2},{3,11},{11,3},{4,12},{12,4},... | collective-permute-start | bytes 147464 | tf_op jit(solution)/shard_map/ppermute | solution.py:246
  53.6 8.6 %copy-start.2 = (bf16[64,1024]{1,0:T(8,128)(2,1)S(1)}, bf16[64,1024]{1,0:T(8,128)(2,1)}, u32[]{:S(2)}) copy-start(bf16[64,1024]{1,0:T(8,128)(2,1)} %param.28) | copy-start | bytes 393220
  53.6 36.0 %all-to-all-start.1 = ((bf16[32,4,512]{2,1,0:T(4,128)(2,1)}), bf16[32,4,512]{2,1,0:T(4,128)(2,1)S(1)}, u32[]{:S(2)}, u32[]{:S(2)}) async-start(bf16[32,4,512]{2,1,0:T(4,128)(2,1)} %shard_map.159), calls=%async_computation.1 | async-start | bytes 262144 | tf_op jit(solution)/shard_map/all_to_all | solution.py:22
  61.5 0.7 copy-start.4
  62.2 0.9 copy-start.3
  63.1 26.5 %copy-start.1 = (f32[4,2,128,128]{3,2,1,0:T(8,128)S(1)}, f32[4,2,128,128]{3,2,1,0:T(8,128)}, u32[]{:S(2)}) copy-start(f32[4,2,128,128]{3,2,1,0:T(8,128)} %state.3) | copy-start | bytes 1572868
  91.9 28.1 %all-to-all-start.2 = ((bf16[32,4,256]{2,1,0:T(4,128)(2,1)}), bf16[32,4,256]{2,1,0:T(4,128)(2,1)S(1)}, u32[]{:S(2)}, u32[]{:S(2)}) async-start(bf16[32,4,256]{2,1,0:T(4,128)(2,1)} %get-tuple-element.12), calls=%async_computation.2 | async-start | bytes 131072 | tf_op jit(solution)/shard_map/all_to_all | solution.py:22
  97.3 9.8 %collective-permute-start.1 = (bf16[128,256]{1,0:T(8,128)(2,1)S(1)}, bf16[128,256]{1,0:T(8,128)(2,1)S(1)}, u32[]{:S(2)}, u32[]{:S(2)}) collective-permute-start(bf16[128,256]{1,0:T(8,128)(2,1)S(1)} %bitcast.60), channel_id=1, source_target_pairs={{0,8},{8,0},{16,24},{24,16},{1,9},{9,1},{17,25},{25,17},{2,10},{10... | collective-permute-start | bytes 196616 | tf_op jit(solution)/shard_map/ppermute | solution.py:205
  100.2 29.3 %collective-permute-start.2 = (bf16[128,256]{1,0:T(8,128)(2,1)S(1)}, bf16[128,256]{1,0:T(8,128)(2,1)S(1)}, u32[]{:S(2)}, u32[]{:S(2)}) collective-permute-start(bf16[128,256]{1,0:T(8,128)(2,1)S(1)} %bitcast.59), channel_id=1, source_target_pairs={{0,16},{8,24},{16,0},{24,8},{1,17},{9,25},{17,1},{25,9},{2,18},{10... | collective-permute-start | bytes 196616 | tf_op jit(solution)/shard_map/ppermute | solution.py:205
  104.3 34.5 %collective-permute-start.3 = (bf16[128,256]{1,0:T(8,128)(2,1)S(1)}, bf16[128,256]{1,0:T(8,128)(2,1)S(1)}, u32[]{:S(2)}, u32[]{:S(2)}) collective-permute-start(bf16[128,256]{1,0:T(8,128)(2,1)S(1)} %bitcast.58), channel_id=1, source_target_pairs={{0,24},{8,16},{16,8},{24,0},{1,25},{9,17},{17,9},{25,1},{2,26},{10... | collective-permute-start | bytes 196616 | tf_op jit(solution)/shard_map/ppermute | solution.py:205
  120.8 13.9 %all-to-all-start.3 = ((bf16[8,64,128]{2,1,0:T(8,128)(2,1)}), bf16[8,64,128]{2,1,0:T(8,128)(2,1)S(1)}, u32[]{:S(2)}, u32[]{:S(2)}) async-start(bf16[8,64,128]{2,1,0:T(8,128)(2,1)} %broadcast_in_dim.49), calls=%async_computation.3 | async-start | bytes 262144 | tf_op jit(solution)/shard_map/all_to_all | solution.py:22
  135.4 7.9 %all-to-all-start.4 = ((bf16[4,64,128]{2,1,0:T(8,128)(2,1)}), bf16[4,64,128]{2,1,0:T(8,128)(2,1)S(1)}, u32[]{:S(2)}, u32[]{:S(2)}) async-start(bf16[4,64,128]{2,1,0:T(8,128)(2,1)} %broadcast_in_dim.54), calls=%async_computation.4 | async-start | bytes 131072 | tf_op jit(solution)/shard_map/all_to_all | solution.py:22
  200.7 16.6 %all-to-all-start.7 = ((bf16[32,8,128]{2,1,0:T(8,128)(2,1)}), bf16[32,8,128]{2,1,0:T(8,128)(2,1)S(1)}, u32[]{:S(2)}, u32[]{:S(2)}) async-start(bf16[32,8,128]{2,1,0:T(8,128)(2,1)} %fusion), calls=%async_computation.7 | async-start | bytes 131072 | tf_op jit(solution)/shard_map/all_to_all | solution.py:22

commit v2 on v1

--- a/solution.py
+++ b/solution.py
@@ -192,22 +192,88 @@
     gained = (w_up.astype(f32) * mixer_gain.astype(f32)[:, None]).astype(bf16)
     both = jnp.concatenate([gained, w_down.T], axis=0)
     both = both.reshape(2 * block, near, wide // near).transpose(1, 0, 2)
-    return [lax.dynamic_index_in_dim(both, me ^ step, 0, keepdims=False) for step in range(near)]
-
-
-def mixer_weights(pieces):
-    near = lax.axis_size(LO)
-    me = lax.axis_index(LO)
-    both, share = pieces[0].shape
-    whole = jnp.zeros((near, both, share), bf16)
-    for step, piece in enumerate(pieces):
+    pieces = []
+    for step in range(near):
+        piece = lax.dynamic_index_in_dim(both, me ^ step, 0, keepdims=False)
         if step:
             piece = lax.ppermute(piece, LO, [(i, i ^ step) for i in range(near)])
-        whole = lax.dynamic_update_slice_in_dim(whole, piece[None], me ^ step, axis=0)
-    block = both // 2
-    up = whole[:, :block].reshape(near * block, share)
-    down_t = whole[:, block:].reshape(near * block, share)
-    return up, down_t
+        pieces.append(piece)
+    return pieces
+
+
+def in_vmem(arrays):
+    return [pltpu.with_memory_space_constraint(x, pltpu.VMEM) for x in arrays]
+
+
+def middle_kernel(arrived, both, sent, kept):
+    own = kept.shape[0]
+    side, place = lax.axis_index("pair"), lax.axis_index("tp")
+    total = both[side].astype(f32)
+    added = arrived[0].astype(f32)
+    for source in range(1, arrived.shape[0]):
+        added = added + arrived[source].astype(f32)
+    block = (total + added).astype(bf16)
+    for target in range(sent.shape[0]):
+        sent[target] = block
+    block = block.astype(f32)
+    chosen = jnp.zeros(kept.shape, f32)
+    for n in range(block.shape[0] // own):
+        chosen = chosen + jnp.where(place == n, block[n * own : (n + 1) * own], 0.0)
+    kept[...] = chosen
+
+
+def middle_rows(arrived, both, near, own):
+    _, block, rows = both.shape
+    arrived = pltpu.with_memory_space_constraint(arrived, pltpu.VMEM)
+    both = pltpu.with_memory_space_constraint(both, pltpu.VMEM)
+    return pl.pallas_call(
+        middle_kernel,
+        out_shape=(pltpu.VMEM((near, block, rows), bf16), pltpu.VMEM((own, rows), f32)),
+    )(arrived, both)
+
+
+def up_kernel(middle, *refs):
+    pieces, sent = refs[:-1], refs[-1]
+    me = lax.axis_index(LO)
+    block = middle.shape[1]
+    total, squares = 0.0, 0.0
+    for step, piece in enumerate(pieces):
+        part = middle[me ^ step]
+        weight = jnp.transpose(piece[:block].astype(f32)).astype(bf16)
+        total = total + dotted(weight, part, 1, 0)
+        part = part.astype(f32)
+        squares = squares + jnp.sum(part * part, axis=0, keepdims=True)
+    tail = jnp.broadcast_to(squares, (8, squares.shape[1])).astype(bf16)
+    share = total.shape[0] // sent.shape[0]
+    for target in range(sent.shape[0]):
+        sent[target, :share] = total[target * share : (target + 1) * share].astype(bf16)
+        sent[target, share:] = tail
+
+
+def up_sums(middle, pieces, far):
+    middle = pltpu.with_memory_space_constraint(middle, pltpu.VMEM)
+    share = pieces[0].shape[1] // far
+    shape = (far, share + 8, middle.shape[2])
+    return pl.pallas_call(up_kernel, out_shape=pltpu.VMEM(shape, bf16))(middle, *in_vmem(pieces))
+
+
+def down_kernel(hidden, *refs):
+    pieces, sent = refs[:-1], refs[-1]
+    me = lax.axis_index(LO)
+    own = sent.shape[1]
+    whole = jnp.concatenate([hidden[n] for n in range(hidden.shape[0])], axis=0)
+    for step, piece in enumerate(pieces):
+        block = piece.shape[0] // 2
+        part = dotted(piece[block:], whole, 1, 0)
+        for n in range(block // own):
+            sent[(me ^ step) * (block // own) + n] = part[n * own : (n + 1) * own].astype(bf16)
+
+
+def down_sums(hidden, pieces, own):
+    hidden = pltpu.with_memory_space_constraint(hidden, pltpu.VMEM)
+    slots = len(pieces) * pieces[0].shape[0] // 2 // own
+    shape = jax.ShapeDtypeStruct((slots, own, hidden.shape[2]), bf16)
+    return pl.pallas_call(down_kernel, out_shape=shape)(hidden, *in_vmem(pieces))
 
 
 def local(
@@ -234,8 +300,6 @@
     width = w_beta.shape[0]
     rows, own = tokens.shape
     block = own * n_tp
-    tp_index = lax.axis_index("tp")
-    side = lax.axis_index("pair")
     columns = heads_here * head_size
     assert heads_here == lax.axis_size("pair")
 
@@ -246,35 +310,28 @@
     taken = lax.ppermute(given, "pair", [(0, 1), (1, 0)])
 
     both = from_everyone(tokens_t, ("pair", "tp")).reshape(2, block, rows)
-    inputs = lax.dynamic_index_in_dim(both, side, 0, keepdims=False).astype(f32)
     sent = partial_sums(both, kept, taken, gates, n_kv, seq_here)
     pieces = mixer_pieces(w_up, w_down, mixer_gain)
     arrived = exchange(sent, KV)
-    up, down_t = mixer_weights(pieces)
-    normed_all, keyed, fresh, decay = delta_update(arrived, state, a_log, dt_bias, head_gain, width, w_beta.shape[1])
+    arrived, pieces[0] = lax.optimization_barrier((arrived, pieces[0]))
+    normed_all, keyed, fresh, decay = delta_update(
+        arrived, state, a_log, dt_bias, head_gain, width, w_beta.shape[1]
+    )
     every = exchange(normed_all, KV).reshape(rows, columns)
     new_state = state_update(state, keyed, fresh, decay)
     head_part = dotted(w_out, every, 0, 1).astype(bf16)
-    attended = from_everyone(head_part, "tp").astype(f32).sum(axis=0)
-    middle_block = (inputs + attended).astype(bf16)
-    middle_own = lax.dynamic_slice_in_dim(middle_block, tp_index * own, own, axis=0)
-
-    middle = from_everyone(middle_block, LO).reshape(n_near * block, rows)
-    middle_f = middle.astype(f32)
-    squares_two = jnp.sum(middle_f * middle_f, axis=0, keepdims=True)
-    hidden_part = dotted(up, middle, 0, 0)
-    far = lax.axis_size("hi")
-    hidden_part = hidden_part.reshape(far, -1, rows)
-    tail = jnp.broadcast_to(squares_two, (far, 8, rows))
-    sent = jnp.concatenate([hidden_part, tail], axis=1).astype(bf16)
+    arrived = from_everyone(head_part, "tp")
+    middle_sent, middle_own = middle_rows(arrived, both, n_near, own)
+    middle_sent, *pieces = lax.optimization_barrier((middle_sent, *pieces))
+    middle = exchange(middle_sent, LO)
+    sent = up_sums(middle, pieces, lax.axis_size("hi"))
     sums = exchange(sent, "hi").astype(f32).sum(axis=0)
     second = lax.rsqrt(sums[-1:] / width + epsilon)
     hidden_own = jnp.square(jax.nn.relu(second * sums[:-8])).astype(bf16)
-    hidden = from_everyone(hidden_own, "hi").reshape(-1, rows)
-    down_part = dotted(down_t, hidden, 1, 0).astype(bf16)
-    arrived = exchange(down_part.reshape(n_near * n_tp, own, rows), NEAR)
-    lowered = arrived.astype(f32).sum(axis=0)
-    mixed = (middle_own.astype(f32) + lowered).astype(bf16).T
+    hidden = from_everyone(hidden_own, "hi")
+    sent = down_sums(hidden, pieces, own)
+    lowered = exchange(sent, NEAR).astype(f32).sum(axis=0)
+    mixed = (middle_own + lowered).astype(bf16).T
     return (mixed, new_state)
 
 

time: 219 us -> 220 us (level)
  blocking collectives: 56.3 us -> 86.6 us
  waiting for transfers between devices: 55.6 us -> 34.4 us
  starting transfers between devices: 91.7 us -> 85.2 us
    all_to_all x2 -> x4, blocking collectives: 56.3 us -> 86.6 us  [exchange(): return lax.all_to_all(x, axis, split_axis=0, concat_axis=0, tiled=True)]
    all_to_all x6 -> x4, waiting for transfers between devices: 54.1 us -> 31.1 us  [exchange(): return lax.all_to_all(x, axis, split_axis=0, concat_axis=0, tiled=True)]
    all_to_all x6 -> x4, starting transfers between devices: 78.9 us -> 72.4 us  [exchange(): return lax.all_to_all(x, axis, split_axis=0, concat_axis=0, tiled=True)]
  transfers between devices with their start and end apart: 10 -> 8, of which waited for: 6 -> 4; matrix products, arithmetic and copies ran while one was open for 1% -> 0% of each run, Pallas kernels for 2% -> 2%
where the time goes in v2:
time: 220 us; the launch traced here: 219 us
  blocking collectives  86.6 us (39%)
  starting transfers between devices  85.2 us (39%)
  waiting for transfers between devices  34.4 us (16%)
  Pallas kernels  6.95 us (3%)
  local copies, waits for them, and re-layouts  4.29 us (2%)
    all_to_all x4, blocking collectives, exchange(): return lax.all_to_all(x, axis, split_axis=0, concat_axis=0, tiled=True)  86.6 us
    all_to_all x4, starting transfers between devices, exchange(): return lax.all_to_all(x, axis, split_axis=0, concat_axis=0, tiled=True)  72.4 us
    all_to_all x4, waiting for transfers between devices, exchange(): return lax.all_to_all(x, axis, split_axis=0, concat_axis=0, tiled=True)  31.1 us
    ppermute x3, starting transfers between devices, mixer_pieces(): piece = lax.ppermute(piece, LO, [(i, i ^ step) for i in range(near)])  9.36 us
  transfers between devices with their start and end apart: 8, of which 4 were waited for; matrix products, arithmetic and copies ran while one was open for 0% of the time, Pallas kernels for 2%

profile of v2, /device:TPU:33, one launch (start us, length us, event | category | flops | bytes accessed | tf_op | source)
XLA Modules:
  0.0 219.3 jit_solution(12340042292753358743)
XLA Ops:
  0.6 0.0 copy-start
  0.6 1.3 broadcast_in_dim.22
  2.0 44.7 %all-to-all-start = ((bf16[16,8,128]{2,1,0:T(8,128)(2,1)}), bf16[16,8,128]{2,1,0:T(8,128)(2,1)S(1)}, u32[]{:S(2)}, u32[]{:S(2)}) async-start(bf16[16,8,128]{2,1,0:T(8,128)(2,1)} %broadcast_in_dim.22), calls=%async_computation | async-start | bytes 65536 | tf_op jit(solution)/shard_map/all_to_all | solution.py:22
  46.7 1.0 shard_map.158
  47.7 3.4 %collective-permute-start = (bf16[64,384]{1,0:T(8,128)(2,1)S(1)}, bf16[64,384]{1,0:T(8,128)(2,1)S(1)}, u32[]{:S(2)}, u32[]{:S(2)}) collective-permute-start(bf16[64,384]{1,0:T(8,128)(2,1)S(1)} %get-tuple-element.19), channel_id=1, source_target_pairs={{0,8},{8,0},{1,9},{9,1},{2,10},{10,2},{3,11},{11,3},{4,12},{12,4},... | collective-permute-start | bytes 147464 | tf_op jit(solution)/shard_map/ppermute | solution.py:310
  51.2 1.5 collective-permute-done.taken
  52.7 0.0 all-to-all-done
  52.7 0.9 shard_map.159
  53.6 0.0 copy-start.2
  53.6 7.9 %all-to-all-start.1 = ((bf16[32,4,512]{2,1,0:T(4,128)(2,1)}), bf16[32,4,512]{2,1,0:T(4,128)(2,1)S(1)}, u32[]{:S(2)}, u32[]{:S(2)}) async-start(bf16[32,4,512]{2,1,0:T(4,128)(2,1)} %shard_map.159), calls=%async_computation.1 | async-start | bytes 262144 | tf_op jit(solution)/shard_map/all_to_all | solution.py:22
  61.5 0.0 copy-start.4
  61.6 0.6 copy-done.4
  62.2 0.0 copy-done.2
  62.2 0.0 copy-start.3
  62.2 0.1 multiply_convert_fusion
  62.3 0.8 copy-done.3
  63.1 0.2 reshape.23
  63.3 0.0 copy-start.1
  63.3 0.5 constant_dynamic-slice_fusion
  63.9 25.7 %all-to-all-done.1.arrived = bf16[32,4,512]{2,1,0:T(4,128)(2,1)S(1)} async-done(((bf16[32,4,512]{2,1,0:T(4,128)(2,1)}), bf16[32,4,512]{2,1,0:T(4,128)(2,1)S(1)}, u32[]{:S(2)}, u32[]{:S(2)}) %all-to-all-start.1) | async-done | bytes 131104 | tf_op jit(solution)/shard_map/all_to_all | solution.py:22
  89.7 0.0 copy-done.1
  89.7 1.6 shard_map.160
  91.2 27.8 %all_to_all.40 = bf16[32,4,256]{2,1,0:T(4,128)(2,1)S(1)} all-to-all(bf16[32,4,256]{2,1,0:T(4,128)(2,1)S(1)} %get-tuple-element.22), channel_id=1, replica_groups=mesh['grp'=2,'hi'=8,'mid'=2,'pair'=2,'tp'=8] {'hi','mid','pair'}, dimensions={0} | all-to-all | bytes 131072 | tf_op jit(solution)/shard_map/all_to_all | solution.py:22
  119.0 0.0 copy-done
  119.1 0.1 fusion
  119.2 0.7 broadcast_in_dim.27
  119.9 7.9 %all-to-all-start.3 = ((bf16[8,64,128]{2,1,0:T(8,128)(2,1)}), bf16[8,64,128]{2,1,0:T(8,128)(2,1)S(1)}, u32[]{:S(2)}, u32[]{:S(2)}) async-start(bf16[8,64,128]{2,1,0:T(8,128)(2,1)} %broadcast_in_dim.27), calls=%async_computation.3 | async-start | bytes 262144 | tf_op jit(solution)/shard_map/all_to_all | solution.py:22
  127.8 2.2 collective-permute-start.1
  130.0 2.1 collective-permute-start.2
  132.1 5.1 %collective-permute-start.3 = (bf16[128,256]{1,0:T(8,128)(2,1)S(1)}, bf16[128,256]{1,0:T(8,128)(2,1)S(1)}, u32[]{:S(2)}, u32[]{:S(2)}) collective-permute-start(bf16[128,256]{1,0:T(8,128)(2,1)S(1)} %bitcast.38), channel_id=1, source_target_pairs={{0,24},{8,16},{16,8},{24,0},{1,25},{9,17},{17,9},{25,1},{2,26},{10... | collective-permute-start | bytes 196616 | tf_op jit(solution)/shard_map/ppermute | solution.py:199
  137.2 0.0 all-to-all-done.3.arrived
  137.2 0.0 collective-permute-done.1.refs_1_
  137.2 0.0 collective-permute-done.2.refs_2_
  137.3 1.8 collective-permute-done.3.refs_3_
  139.1 8.7 %all_to_all.41.middle = bf16[4,64,128]{2,1,0:T(8,128)(2,1)S(1)} all-to-all(bf16[4,64,128]{2,1,0:T(8,128)(2,1)S(1)} %get-tuple-element.26), channel_id=1, replica_groups=mesh['grp'=2,'hi'=8,'mid'=2,'pair'=2,'tp'=8] {'mid','pair'}, dimensions={0} | all-to-all | bytes 131072 | tf_op jit(solution)/shard_map/all_to_all | solution.py:22
  147.8 0.3 shard_map.162
  148.1 24.1 %all_to_all.42 = bf16[8,40,128]{2,1,0:T(8,128)(2,1)S(1)} all-to-all(bf16[8,40,128]{2,1,0:T(8,128)(2,1)S(1)} %shard_map.162), channel_id=1, replica_groups=mesh['grp'=2,'hi'=8,'mid'=2,'pair'=2,'tp'=8] {'hi'}, dimensions={0} | all-to-all | bytes 163840 | tf_op jit(solution)/shard_map/all_to_all | solution.py:22
  172.2 26.1 %all_to_all.43.hidden = bf16[8,32,128]{2,1,0:T(8,128)(2,1)S(1)} all-to-all(bf16[8,32,128]{2,1,0:T(8,128)(2,1)S(1)} %broadcast_in_dim.28), channel_id=1, replica_groups=mesh['grp'=2,'hi'=8,'mid'=2,'pair'=2,'tp'=8] {'hi'}, dimensions={0} | all-to-all | bytes 131072 | tf_op jit(solution)/shard_map/all_to_all | solution.py:22
  198.3 0.8 shard_map.163
  199.1 12.0 %all-to-all-start.7 = ((bf16[32,8,128]{2,1,0:T(8,128)(2,1)}), bf16[32,8,128]{2,1,0:T(8,128)(2,1)S(1)}, u32[]{:S(2)}, u32[]{:S(2)}) async-start(bf16[32,8,128]{2,1,0:T(8,128)(2,1)} %shard_map.163), calls=%async_computation.7 | async-start | bytes 131072 | tf_op jit(solution)/shard_map/all_to_all | solution.py:22
  211.1 2.3 %shard_map.164 = f32[4,2,128,128]{3,2,1,0:T(8,128)} custom-call(f32[4,2,128,128]{3,2,1,0:T(8,128)} %state.3, f32[2,4,128]{2,1,0:T(4,128)S(1)} %get-tuple-element.31.keyed, f32[2,4,128]{2,1,0:T(4,128)S(1)} %get-tuple-element.32.fresh, f32[2,4,128]{2,1,0:T(4,128)S(1)} %get-tuple-element.33.decay), custom_call_target="tpu_custom_call" | custom-call | tf_op jit(solution)/shard_map/pallas_call | solution.py:185
  213.3 5.4 %all-to-all-done.7 = bf16[32,8,128]{2,1,0:T(8,128)(2,1)S(1)} async-done(((bf16[32,8,128]{2,1,0:T(8,128)(2,1)}), bf16[32,8,128]{2,1,0:T(8,128)(2,1)S(1)}, u32[]{:S(2)}, u32[]{:S(2)}) %all-to-all-start.7) | async-done | bytes 65568 | tf_op jit(solution)/shard_map/all_to_all | solution.py:22
  218.8 0.6 fusion.4
  (13 shorter events, 0.2 us)
Async XLA Ops:
  0.6 118.4 %copy-start = (bf16[256,64]{0,1:T(8,128)(2,1)S(1)}, bf16[256,64]{0,1:T(8,128)(2,1)}, u32[]{:S(2)}) copy-start(bf16[256,64]{0,1:T(8,128)(2,1)} %param.26) | copy-start | bytes 98308
  2.0 50.7 %all-to-all-start = ((bf16[16,8,128]{2,1,0:T(8,128)(2,1)}), bf16[16,8,128]{2,1,0:T(8,128)(2,1)S(1)}, u32[]{:S(2)}, u32[]{:S(2)}) async-start(bf16[16,8,128]{2,1,0:T(8,128)(2,1)} %broadcast_in_dim.22), calls=%async_computation | async-start | bytes 65536 | tf_op jit(solution)/shard_map/all_to_all | solution.py:22
  47.7 5.0 %collective-permute-start = (bf16[64,384]{1,0:T(8,128)(2,1)S(1)}, bf16[64,384]{1,0:T(8,128)(2,1)S(1)}, u32[]{:S(2)}, u32[]{:S(2)}) collective-permute-start(bf16[64,384]{1,0:T(8,128)(2,1)S(1)} %get-tuple-element.19), channel_id=1, source_target_pairs={{0,8},{8,0},{1,9},{9,1},{2,10},{10,2},{3,11},{11,3},{4,12},{12,4},... | collective-permute-start | bytes 147464 | tf_op jit(solution)/shard_map/ppermute | solution.py:310
  53.6 8.6 %copy-start.2 = (bf16[64,1024]{1,0:T(8,128)(2,1)S(1)}, bf16[64,1024]{1,0:T(8,128)(2,1)}, u32[]{:S(2)}) copy-start(bf16[64,1024]{1,0:T(8,128)(2,1)} %param.28) | copy-start | bytes 393220
  53.6 36.0 %all-to-all-start.1 = ((bf16[32,4,512]{2,1,0:T(4,128)(2,1)}), bf16[32,4,512]{2,1,0:T(4,128)(2,1)S(1)}, u32[]{:S(2)}, u32[]{:S(2)}) async-start(bf16[32,4,512]{2,1,0:T(4,128)(2,1)} %shard_map.159), calls=%async_computation.1 | async-start | bytes 262144 | tf_op jit(solution)/shard_map/all_to_all | solution.py:22
  61.5 0.7 copy-start.4
  62.2 0.9 copy-start.3
  63.3 26.3 %copy-start.1 = (f32[4,2,128,128]{3,2,1,0:T(8,128)S(1)}, f32[4,2,128,128]{3,2,1,0:T(8,128)}, u32[]{:S(2)}) copy-start(f32[4,2,128,128]{3,2,1,0:T(8,128)} %state.3) | copy-start | bytes 1572868
  119.9 17.3 %all-to-all-start.3 = ((bf16[8,64,128]{2,1,0:T(8,128)(2,1)}), bf16[8,64,128]{2,1,0:T(8,128)(2,1)S(1)}, u32[]{:S(2)}, u32[]{:S(2)}) async-start(bf16[8,64,128]{2,1,0:T(8,128)(2,1)} %broadcast_in_dim.27), calls=%async_computation.3 | async-start | bytes 262144 | tf_op jit(solution)/shard_map/all_to_all | solution.py:22
  127.8 9.5 %collective-permute-start.1 = (bf16[128,256]{1,0:T(8,128)(2,1)S(1)}, bf16[128,256]{1,0:T(8,128)(2,1)S(1)}, u32[]{:S(2)}, u32[]{:S(2)}) collective-permute-start(bf16[128,256]{1,0:T(8,128)(2,1)S(1)} %bitcast.36), channel_id=1, source_target_pairs={{0,8},{8,0},{16,24},{24,16},{1,9},{9,1},{17,25},{25,17},{2,10},{10... | collective-permute-start | bytes 196616 | tf_op jit(solution)/shard_map/ppermute | solution.py:199
  130.0 7.3 %collective-permute-start.2 = (bf16[128,256]{1,0:T(8,128)(2,1)S(1)}, bf16[128,256]{1,0:T(8,128)(2,1)S(1)}, u32[]{:S(2)}, u32[]{:S(2)}) collective-permute-start(bf16[128,256]{1,0:T(8,128)(2,1)S(1)} %bitcast.37), channel_id=1, source_target_pairs={{0,16},{8,24},{16,0},{24,8},{1,17},{9,25},{17,1},{25,9},{2,18},{10... | collective-permute-start | bytes 196616 | tf_op jit(solution)/shard_map/ppermute | solution.py:199
  132.1 6.9 %collective-permute-start.3 = (bf16[128,256]{1,0:T(8,128)(2,1)S(1)}, bf16[128,256]{1,0:T(8,128)(2,1)S(1)}, u32[]{:S(2)}, u32[]{:S(2)}) collective-permute-start(bf16[128,256]{1,0:T(8,128)(2,1)S(1)} %bitcast.38), channel_id=1, source_target_pairs={{0,24},{8,16},{16,8},{24,0},{1,25},{9,17},{17,9},{25,1},{2,26},{10... | collective-permute-start | bytes 196616 | tf_op jit(solution)/shard_map/ppermute | solution.py:199
  199.1 19.6 %all-to-all-start.7 = ((bf16[32,8,128]{2,1,0:T(8,128)(2,1)}), bf16[32,8,128]{2,1,0:T(8,128)(2,1)S(1)}, u32[]{:S(2)}, u32[]{:S(2)}) async-start(bf16[32,8,128]{2,1,0:T(8,128)(2,1)} %shard_map.163), calls=%async_computation.7 | async-start | bytes 131072 | tf_op jit(solution)/shard_map/all_to_all | solution.py:22

commit v3 on v2

--- a/solution.py
+++ b/solution.py
@@ -10,6 +10,7 @@
 
 
 epsilon = 1e-06
+TAIL = 64
 bf16 = jnp.bfloat16
 f32 = jnp.float32
 KV = ("hi", "mid", "pair")
@@ -32,8 +33,8 @@
 
 
 def delta_kernel(arrived, state, a_log, dt_bias, head_gain, normed_all, keyed_out, fresh_out, decay_out, *, width, all_heads):
-    n_kv, seq, _ = arrived.shape
-    heads = state.shape[1]
+    n_kv = arrived.shape[0]
+    seq, heads = state.shape[:2]
     size = state.shape[3]
     main = 3 * size
     sums = []
@@ -42,16 +43,18 @@
         for source in range(head + heads, n_kv, heads):
             total = total + arrived[source].astype(f32)
         sums.append(total)
-    gates = sums[0][:, main:]
+    ends = sums[0][:, 2 * main :]
     for total in sums[1:]:
-        gates = gates + total[:, main:]
+        ends = ends + total[:, 2 * main :]
+    gates = jnp.concatenate([ends[:, :TAIL], ends[:, TAIL:]], axis=0)
+    sums = [jnp.concatenate([x[:, :main], x[:, main : 2 * main]], axis=0) for x in sums]
     tp_index = lax.axis_index("tp")
     lane = lax.broadcasted_iota(jnp.int32, gates.shape, 1)
     at = lambda n: jnp.sum(jnp.where(lane == n, gates, 0.0), axis=1, keepdims=True)
     first = lax.rsqrt(at(2 * all_heads) / width + epsilon)
     normed = []
     for head in range(heads):
-        pre = first * sums[head][:, :main]
+        pre = first * sums[head]
         query, key, value = (pre[:, n * size : (n + 1) * size] for n in range(3))
         query = query * lax.rsqrt(jnp.sum(query * query, axis=1, keepdims=True) + epsilon)
         key = key * lax.rsqrt(jnp.sum(key * key, axis=1, keepdims=True) + epsilon)
@@ -95,8 +98,8 @@
 
 
 def delta_update(arrived, state, a_log, dt_bias, head_gain, width, all_heads):
-    n_kv, seq, _ = arrived.shape
-    heads, size = state.shape[1:3]
+    n_kv = arrived.shape[0]
+    seq, heads, size = state.shape[:3]
     small = pltpu.VMEM((heads, seq, size), f32)
     arrived = pltpu.with_memory_space_constraint(arrived, pltpu.VMEM)
     state = pltpu.with_memory_space_constraint(state, pltpu.VMEM)
@@ -154,7 +157,7 @@
 
 
 def sums_kernel(both, kept, taken, gates, sent):
-    n_kv, seq, columns = sent.shape
+    n_kv, half, _ = sent.shape
     side = lax.axis_index("pair")
     mine = jnp.transpose(both[side].astype(f32))
     other = jnp.transpose(both[1 - side].astype(f32))
@@ -162,21 +165,28 @@
     mine = mine.astype(bf16)
     main = dotted(mine, kept[...], 1, 0) + dotted(other.astype(bf16), taken[...], 1, 0)
     extra = dotted(mine, gates[...], 1, 0)
-    spare = columns - main.shape[1] - extra.shape[1] - 1
-    tail = jnp.concatenate([extra, squares, jnp.zeros((mine.shape[0], spare), f32)], axis=1)
-    whole = jnp.concatenate([main, tail], axis=1)
+    gap = jnp.zeros((mine.shape[0], TAIL - extra.shape[1] - 1), f32)
+    tail = jnp.concatenate([extra, squares, gap], axis=1)
+    blank = jnp.zeros_like(tail)
+    upper = jnp.concatenate([main, tail, blank], axis=1)
+    lower = jnp.concatenate([blank, tail], axis=1)
+    width = main.shape[1]
     for target in range(n_kv):
-        sent[target] = whole[target * seq : (target + 1) * seq].astype(bf16)
+        at = 2 * target * half
+        top, low = slice(at, at + half), slice(at + half, at + 2 * half)
+        ends = upper[top, width:] + lower[low]
+        sent[target] = jnp.concatenate([upper[top, :width], main[low], ends], axis=1).astype(bf16)
 
 
 def partial_sums(both, kept, taken, gates, n_kv, seq):
     whole = pl.BlockSpec(memory_space=pltpu.VMEM)
-    columns = kept.shape[1] + 128
+    assert seq % 2 == 0 and gates.shape[1] < TAIL
+    columns = 2 * (kept.shape[1] + TAIL)
     near = [pltpu.with_memory_space_constraint(x, pltpu.VMEM) for x in (both, kept, taken, gates)]
     return pl.pallas_call(
         sums_kernel,
         in_specs=[whole] * 4,
-        out_shape=jax.ShapeDtypeStruct((n_kv, seq, columns), bf16),
+        out_shape=jax.ShapeDtypeStruct((n_kv, seq // 2, columns), bf16),
     )(*near)
 
 

time: 220 us -> 219 us (level)
  no operation moved by 1% of the time
where the time goes in v3:
time: 219 us; the launch traced here: 218 us
  blocking collectives  86.7 us (40%)
  starting transfers between devices  85.1 us (39%)
  waiting for transfers between devices  32.8 us (15%)
  Pallas kernels  7.14 us (3%)
  local copies, waits for them, and re-layouts  4.29 us (2%)
    all_to_all x4, blocking collectives, exchange(): return lax.all_to_all(x, axis, split_axis=0, concat_axis=0, tiled=True)  86.7 us
    all_to_all x4, starting transfers between devices, exchange(): return lax.all_to_all(x, axis, split_axis=0, concat_axis=0, tiled=True)  72.3 us
    all_to_all x4, waiting for transfers between devices, exchange(): return lax.all_to_all(x, axis, split_axis=0, concat_axis=0, tiled=True)  29.5 us
    ppermute x3, starting transfers between devices, mixer_pieces(): piece = lax.ppermute(piece, LO, [(i, i ^ step) for i in range(near)])  9.36 us
  transfers between devices with their start and end apart: 8, of which 4 were waited for; matrix products, arithmetic and copies ran while one was open for 0% of the time, Pallas kernels for 2%

profile of v3, /device:TPU:33, one launch (start us, length us, event | category | flops | bytes accessed | tf_op | source)
XLA Modules:
  0.0 217.8 jit_solution(10736473975888307924)
XLA Ops:
  0.6 0.0 copy-start
  0.6 1.3 broadcast_in_dim.22
  2.0 44.7 %all-to-all-start = ((bf16[16,8,128]{2,1,0:T(8,128)(2,1)}), bf16[16,8,128]{2,1,0:T(8,128)(2,1)S(1)}, u32[]{:S(2)}, u32[]{:S(2)}) async-start(bf16[16,8,128]{2,1,0:T(8,128)(2,1)} %broadcast_in_dim.22), calls=%async_computation | async-start | bytes 65536 | tf_op jit(solution)/shard_map/all_to_all | solution.py:23
  46.7 1.0 shard_map.158
  47.7 3.4 %collective-permute-start = (bf16[64,384]{1,0:T(8,128)(2,1)S(1)}, bf16[64,384]{1,0:T(8,128)(2,1)S(1)}, u32[]{:S(2)}, u32[]{:S(2)}) collective-permute-start(bf16[64,384]{1,0:T(8,128)(2,1)S(1)} %get-tuple-element.19), channel_id=1, source_target_pairs={{0,8},{8,0},{1,9},{9,1},{2,10},{10,2},{3,11},{11,3},{4,12},{12,4},... | collective-permute-start | bytes 147464 | tf_op jit(solution)/shard_map/ppermute | solution.py:320
  51.2 1.5 collective-permute-done.taken
  52.7 0.0 all-to-all-done
  52.7 1.0 shard_map.159
  53.7 0.0 copy-start.2
  53.7 7.9 %all-to-all-start.1 = ((bf16[32,2,896]{2,1,0:T(2,128)(2,1)}), bf16[32,2,896]{2,1,0:T(2,128)(2,1)S(1)}, u32[]{:S(2)}, u32[]{:S(2)}) async-start(bf16[32,2,896]{2,1,0:T(2,128)(2,1)} %shard_map.159), calls=%async_computation.1 | async-start | bytes 229376 | tf_op jit(solution)/shard_map/all_to_all | solution.py:23
  61.6 0.0 copy-start.4
  61.6 0.6 copy-done.4
  62.3 0.0 copy-done.2
  62.3 0.0 copy-start.3
  62.3 0.1 multiply_convert_fusion
  62.4 0.8 copy-done.3
  63.2 0.2 reshape.23
  63.4 0.0 copy-start.1
  63.4 0.5 constant_dynamic-slice_fusion
  64.0 24.1 %all-to-all-done.1.arrived = bf16[32,2,896]{2,1,0:T(2,128)(2,1)S(1)} async-done(((bf16[32,2,896]{2,1,0:T(2,128)(2,1)}), bf16[32,2,896]{2,1,0:T(2,128)(2,1)S(1)}, u32[]{:S(2)}, u32[]{:S(2)}) %all-to-all-start.1) | async-done | bytes 114720 | tf_op jit(solution)/shard_map/all_to_all | solution.py:23
  88.1 0.0 copy-done.1
  88.1 1.7 shard_map.160
  89.8 27.9 %all_to_all.40 = bf16[32,4,256]{2,1,0:T(4,128)(2,1)S(1)} all-to-all(bf16[32,4,256]{2,1,0:T(4,128)(2,1)S(1)} %get-tuple-element.22), channel_id=1, replica_groups=mesh['grp'=2,'hi'=8,'mid'=2,'pair'=2,'tp'=8] {'hi','mid','pair'}, dimensions={0} | all-to-all | bytes 131072 | tf_op jit(solution)/shard_map/all_to_all | solution.py:23
  117.7 0.0 copy-done
  117.7 0.1 fusion
  117.9 0.7 broadcast_in_dim.27
  118.6 7.9 %all-to-all-start.3 = ((bf16[8,64,128]{2,1,0:T(8,128)(2,1)}), bf16[8,64,128]{2,1,0:T(8,128)(2,1)S(1)}, u32[]{:S(2)}, u32[]{:S(2)}) async-start(bf16[8,64,128]{2,1,0:T(8,128)(2,1)} %broadcast_in_dim.27), calls=%async_computation.3 | async-start | bytes 262144 | tf_op jit(solution)/shard_map/all_to_all | solution.py:23
  126.5 2.0 collective-permute-start.1
  128.4 2.4 %collective-permute-start.2 = (bf16[128,256]{1,0:T(8,128)(2,1)S(1)}, bf16[128,256]{1,0:T(8,128)(2,1)S(1)}, u32[]{:S(2)}, u32[]{:S(2)}) collective-permute-start(bf16[128,256]{1,0:T(8,128)(2,1)S(1)} %bitcast.37), channel_id=1, source_target_pairs={{0,16},{8,24},{16,0},{24,8},{1,17},{9,25},{17,1},{25,9},{2,18},{10... | collective-permute-start | bytes 196616 | tf_op jit(solution)/shard_map/ppermute | solution.py:209
  130.8 5.0 %collective-permute-start.3 = (bf16[128,256]{1,0:T(8,128)(2,1)S(1)}, bf16[128,256]{1,0:T(8,128)(2,1)S(1)}, u32[]{:S(2)}, u32[]{:S(2)}) collective-permute-start(bf16[128,256]{1,0:T(8,128)(2,1)S(1)} %bitcast.38), channel_id=1, source_target_pairs={{0,24},{8,16},{16,8},{24,0},{1,25},{9,17},{17,9},{25,1},{2,26},{10... | collective-permute-start | bytes 196616 | tf_op jit(solution)/shard_map/ppermute | solution.py:209
  135.9 0.0 all-to-all-done.3.arrived
  135.9 0.0 collective-permute-done.1.refs_1_
  135.9 0.0 collective-permute-done.2.refs_2_
  136.0 1.8 collective-permute-done.3.refs_3_
  137.8 8.7 %all_to_all.41.middle = bf16[4,64,128]{2,1,0:T(8,128)(2,1)S(1)} all-to-all(bf16[4,64,128]{2,1,0:T(8,128)(2,1)S(1)} %get-tuple-element.26), channel_id=1, replica_groups=mesh['grp'=2,'hi'=8,'mid'=2,'pair'=2,'tp'=8] {'mid','pair'}, dimensions={0} | all-to-all | bytes 131072 | tf_op jit(solution)/shard_map/all_to_all | solution.py:23
  146.5 0.3 shard_map.162
  146.8 24.1 %all_to_all.42 = bf16[8,40,128]{2,1,0:T(8,128)(2,1)S(1)} all-to-all(bf16[8,40,128]{2,1,0:T(8,128)(2,1)S(1)} %shard_map.162), channel_id=1, replica_groups=mesh['grp'=2,'hi'=8,'mid'=2,'pair'=2,'tp'=8] {'hi'}, dimensions={0} | all-to-all | bytes 163840 | tf_op jit(solution)/shard_map/all_to_all | solution.py:23
  170.9 26.1 %all_to_all.43.hidden = bf16[8,32,128]{2,1,0:T(8,128)(2,1)S(1)} all-to-all(bf16[8,32,128]{2,1,0:T(8,128)(2,1)S(1)} %broadcast_in_dim.28), channel_id=1, replica_groups=mesh['grp'=2,'hi'=8,'mid'=2,'pair'=2,'tp'=8] {'hi'}, dimensions={0} | all-to-all | bytes 131072 | tf_op jit(solution)/shard_map/all_to_all | solution.py:23
  197.0 0.8 shard_map.163
  197.8 11.8 %all-to-all-start.7 = ((bf16[32,8,128]{2,1,0:T(8,128)(2,1)}), bf16[32,8,128]{2,1,0:T(8,128)(2,1)S(1)}, u32[]{:S(2)}, u32[]{:S(2)}) async-start(bf16[32,8,128]{2,1,0:T(8,128)(2,1)} %shard_map.163), calls=%async_computation.7 | async-start | bytes 131072 | tf_op jit(solution)/shard_map/all_to_all | solution.py:23
  209.6 2.3 %shard_map.164 = f32[4,2,128,128]{3,2,1,0:T(8,128)} custom-call(f32[4,2,128,128]{3,2,1,0:T(8,128)} %state.3, f32[2,4,128]{2,1,0:T(4,128)S(1)} %get-tuple-element.31.keyed, f32[2,4,128]{2,1,0:T(4,128)S(1)} %get-tuple-element.32.fresh, f32[2,4,128]{2,1,0:T(4,128)S(1)} %get-tuple-element.33.decay), custom_call_target="tpu_custom_call" | custom-call | tf_op jit(solution)/shard_map/pallas_call | solution.py:195
  211.9 5.4 %all-to-all-done.7 = bf16[32,8,128]{2,1,0:T(8,128)(2,1)S(1)} async-done(((bf16[32,8,128]{2,1,0:T(8,128)(2,1)}), bf16[32,8,128]{2,1,0:T(8,128)(2,1)S(1)}, u32[]{:S(2)}, u32[]{:S(2)}) %all-to-all-start.7) | async-done | bytes 65568 | tf_op jit(solution)/shard_map/all_to_all | solution.py:23
  217.3 0.6 fusion.4
  (13 shorter events, 0.2 us)
Async XLA Ops:
  0.6 117.1 %copy-start = (bf16[256,64]{0,1:T(8,128)(2,1)S(1)}, bf16[256,64]{0,1:T(8,128)(2,1)}, u32[]{:S(2)}) copy-start(bf16[256,64]{0,1:T(8,128)(2,1)} %param.26) | copy-start | bytes 98308
  2.0 50.7 %all-to-all-start = ((bf16[16,8,128]{2,1,0:T(8,128)(2,1)}), bf16[16,8,128]{2,1,0:T(8,128)(2,1)S(1)}, u32[]{:S(2)}, u32[]{:S(2)}) async-start(bf16[16,8,128]{2,1,0:T(8,128)(2,1)} %broadcast_in_dim.22), calls=%async_computation | async-start | bytes 65536 | tf_op jit(solution)/shard_map/all_to_all | solution.py:23
  47.7 5.0 %collective-permute-start = (bf16[64,384]{1,0:T(8,128)(2,1)S(1)}, bf16[64,384]{1,0:T(8,128)(2,1)S(1)}, u32[]{:S(2)}, u32[]{:S(2)}) collective-permute-start(bf16[64,384]{1,0:T(8,128)(2,1)S(1)} %get-tuple-element.19), channel_id=1, source_target_pairs={{0,8},{8,0},{1,9},{9,1},{2,10},{10,2},{3,11},{11,3},{4,12},{12,4},... | collective-permute-start | bytes 147464 | tf_op jit(solution)/shard_map/ppermute | solution.py:320
  53.7 8.6 %copy-start.2 = (bf16[64,1024]{1,0:T(8,128)(2,1)S(1)}, bf16[64,1024]{1,0:T(8,128)(2,1)}, u32[]{:S(2)}) copy-start(bf16[64,1024]{1,0:T(8,128)(2,1)} %param.28) | copy-start | bytes 393220
  53.7 34.4 %all-to-all-start.1 = ((bf16[32,2,896]{2,1,0:T(2,128)(2,1)}), bf16[32,2,896]{2,1,0:T(2,128)(2,1)S(1)}, u32[]{:S(2)}, u32[]{:S(2)}) async-start(bf16[32,2,896]{2,1,0:T(2,128)(2,1)} %shard_map.159), calls=%async_computation.1 | async-start | bytes 229376 | tf_op jit(solution)/shard_map/all_to_all | solution.py:23
  61.6 0.7 copy-start.4
  62.3 0.9 copy-start.3
  63.4 24.7 %copy-start.1 = (f32[4,2,128,128]{3,2,1,0:T(8,128)S(1)}, f32[4,2,128,128]{3,2,1,0:T(8,128)}, u32[]{:S(2)}) copy-start(f32[4,2,128,128]{3,2,1,0:T(8,128)} %state.3) | copy-start | bytes 1572868
  118.6 17.3 %all-to-all-start.3 = ((bf16[8,64,128]{2,1,0:T(8,128)(2,1)}), bf16[8,64,128]{2,1,0:T(8,128)(2,1)S(1)}, u32[]{:S(2)}, u32[]{:S(2)}) async-start(bf16[8,64,128]{2,1,0:T(8,128)(2,1)} %broadcast_in_dim.27), calls=%async_computation.3 | async-start | bytes 262144 | tf_op jit(solution)/shard_map/all_to_all | solution.py:23
  126.5 9.5 %collective-permute-start.1 = (bf16[128,256]{1,0:T(8,128)(2,1)S(1)}, bf16[128,256]{1,0:T(8,128)(2,1)S(1)}, u32[]{:S(2)}, u32[]{:S(2)}) collective-permute-start(bf16[128,256]{1,0:T(8,128)(2,1)S(1)} %bitcast.36), channel_id=1, source_target_pairs={{0,8},{8,0},{16,24},{24,16},{1,9},{9,1},{17,25},{25,17},{2,10},{10... | collective-permute-start | bytes 196616 | tf_op jit(solution)/shard_map/ppermute | solution.py:209
  128.4 7.5 %collective-permute-start.2 = (bf16[128,256]{1,0:T(8,128)(2,1)S(1)}, bf16[128,256]{1,0:T(8,128)(2,1)S(1)}, u32[]{:S(2)}, u32[]{:S(2)}) collective-permute-start(bf16[128,256]{1,0:T(8,128)(2,1)S(1)} %bitcast.37), channel_id=1, source_target_pairs={{0,16},{8,24},{16,0},{24,8},{1,17},{9,25},{17,1},{25,9},{2,18},{10... | collective-permute-start | bytes 196616 | tf_op jit(solution)/shard_map/ppermute | solution.py:209
  130.8 6.9 %collective-permute-start.3 = (bf16[128,256]{1,0:T(8,128)(2,1)S(1)}, bf16[128,256]{1,0:T(8,128)(2,1)S(1)}, u32[]{:S(2)}, u32[]{:S(2)}) collective-permute-start(bf16[128,256]{1,0:T(8,128)(2,1)S(1)} %bitcast.38), channel_id=1, source_target_pairs={{0,24},{8,16},{16,8},{24,0},{1,25},{9,17},{17,9},{25,1},{2,26},{10... | collective-permute-start | bytes 196616 | tf_op jit(solution)/shard_map/ppermute | solution.py:209
  197.8 19.4 %all-to-all-start.7 = ((bf16[32,8,128]{2,1,0:T(8,128)(2,1)}), bf16[32,8,128]{2,1,0:T(8,128)(2,1)S(1)}, u32[]{:S(2)}, u32[]{:S(2)}) async-start(bf16[32,8,128]{2,1,0:T(8,128)(2,1)} %shard_map.163), calls=%async_computation.7 | async-start | bytes 131072 | tf_op jit(solution)/shard_map/all_to_all | solution.py:23

commit v4 on v3

--- a/solution.py
+++ b/solution.py
@@ -195,16 +195,45 @@
     return pl.pallas_call(state_kernel, out_shape=jax.ShapeDtypeStruct(state.shape, f32))(state, *small)
 
 
+def pieces_kernel(w_up, w_down_t, gain, *refs):
+    near = lax.axis_size(LO)
+    pieces, held, held_gain, arrivals = refs[:near], refs[near], refs[near + 1], refs[near + 2]
+    me = lax.axis_index(LO)
+    block = w_up.shape[0]
+    share = pieces[0].shape[1]
+    copies = [pltpu.make_async_copy(gain, held_gain, arrivals.at[2 * near])]
+    for step, piece in enumerate(pieces):
+        cut = pl.ds(pl.multiple_of((me ^ step) * share, share), share)
+        copies.append(pltpu.make_async_copy(w_up.at[:, cut], held.at[step], arrivals.at[2 * step]))
+        copies.append(
+            pltpu.make_async_copy(w_down_t.at[:, cut], piece.at[pl.ds(block, block)], arrivals.at[2 * step + 1])
+        )
+    for copy in copies:
+        copy.start()
+    for copy in copies:
+        copy.wait()
+    wide = jnp.broadcast_to(held_gain[...].astype(f32), (8, block))
+    column = jnp.transpose(wide)[:, :1]
+    for step, piece in enumerate(pieces):
+        piece[:block] = (held[step].astype(f32) * column).astype(bf16)
+
+
 def mixer_pieces(w_up, w_down, mixer_gain):
     near = lax.axis_size(LO)
-    me = lax.axis_index(LO)
     block, wide = w_up.shape
-    gained = (w_up.astype(f32) * mixer_gain.astype(f32)[:, None]).astype(bf16)
-    both = jnp.concatenate([gained, w_down.T], axis=0)
-    both = both.reshape(2 * block, near, wide // near).transpose(1, 0, 2)
+    share = wide // near
+    cut = pl.pallas_call(
+        pieces_kernel,
+        in_specs=[pl.BlockSpec(memory_space=pl.ANY)] * 3,
+        out_shape=tuple(pltpu.VMEM((2 * block, share), bf16) for _ in range(near)),
+        scratch_shapes=[
+            pltpu.VMEM((near, block, share), bf16),
+            pltpu.VMEM((1, block), bf16),
+            pltpu.SemaphoreType.DMA((2 * near + 1,)),
+        ],
+    )(w_up, w_down.T, mixer_gain[None])
     pieces = []
-    for step in range(near):
-        piece = lax.dynamic_index_in_dim(both, me ^ step, 0, keepdims=False)
+    for step, piece in enumerate(cut):
         if step:
             piece = lax.ppermute(piece, LO, [(i, i ^ step) for i in range(near)])
         pieces.append(piece)

time: 219 us -> 219 us (level)
  local copies, waits for them, and re-layouts: 4.29 us -> 2.05 us
where the time goes in v4:
time: 219 us; the launch traced here: 218 us
  blocking collectives  86.7 us (40%)
  starting transfers between devices  85.1 us (39%)
  waiting for transfers between devices  34.1 us (16%)
  Pallas kernels  8.28 us (4%)
    all_to_all x4, blocking collectives, exchange(): return lax.all_to_all(x, axis, split_axis=0, concat_axis=0, tiled=True)  86.7 us
    all_to_all x4, starting transfers between devices, exchange(): return lax.all_to_all(x, axis, split_axis=0, concat_axis=0, tiled=True)  72.3 us
    all_to_all x4, waiting for transfers between devices, exchange(): return lax.all_to_all(x, axis, split_axis=0, concat_axis=0, tiled=True)  30.7 us
    ppermute x3, starting transfers between devices, mixer_pieces(): piece = lax.ppermute(piece, LO, [(i, i ^ step) for i in range(near)])  9.35 us
  transfers between devices with their start and end apart: 8, of which 4 were waited for; matrix products, arithmetic and copies ran while one was open for 0% of the time, Pallas kernels for 2%

profile of v4, /device:TPU:33, one launch (start us, length us, event | category | flops | bytes accessed | tf_op | source)
XLA Modules:
  0.0 217.8 jit_solution(16140769179865453875)
XLA Ops:
  0.6 0.0 copy-start
  0.6 1.3 broadcast_in_dim.24
  2.0 0.0 copy-start.1
  2.0 44.9 %all-to-all-start = ((bf16[16,8,128]{2,1,0:T(8,128)(2,1)}), bf16[16,8,128]{2,1,0:T(8,128)(2,1)S(1)}, u32[]{:S(2)}, u32[]{:S(2)}) async-start(bf16[16,8,128]{2,1,0:T(8,128)(2,1)} %broadcast_in_dim.24), calls=%async_computation | async-start | bytes 65536 | tf_op jit(solution)/shard_map/all_to_all | solution.py:23
  46.8 1.0 shard_map.158
  47.9 3.4 %collective-permute-start = (bf16[64,384]{1,0:T(8,128)(2,1)S(1)}, bf16[64,384]{1,0:T(8,128)(2,1)S(1)}, u32[]{:S(2)}, u32[]{:S(2)}) collective-permute-start(bf16[64,384]{1,0:T(8,128)(2,1)S(1)} %get-tuple-element.23), channel_id=1, source_target_pairs={{0,8},{8,0},{1,9},{9,1},{2,10},{10,2},{3,11},{11,3},{4,12},{12,4},... | collective-permute-start | bytes 147464 | tf_op jit(solution)/shard_map/ppermute | solution.py:349
  51.3 1.5 collective-permute-done.taken
  52.8 0.0 all-to-all-done
  52.8 1.0 shard_map.159
  53.8 7.7 %all-to-all-start.1 = ((bf16[32,2,896]{2,1,0:T(2,128)(2,1)}), bf16[32,2,896]{2,1,0:T(2,128)(2,1)S(1)}, u32[]{:S(2)}, u32[]{:S(2)}) async-start(bf16[32,2,896]{2,1,0:T(2,128)(2,1)} %shard_map.159), calls=%async_computation.1 | async-start | bytes 229376 | tf_op jit(solution)/shard_map/all_to_all | solution.py:23
  61.6 1.1 shard_map.160
  62.7 25.4 %all-to-all-done.1.arrived = bf16[32,2,896]{2,1,0:T(2,128)(2,1)S(1)} async-done(((bf16[32,2,896]{2,1,0:T(2,128)(2,1)}), bf16[32,2,896]{2,1,0:T(2,128)(2,1)S(1)}, u32[]{:S(2)}, u32[]{:S(2)}) %all-to-all-start.1) | async-done | bytes 114720 | tf_op jit(solution)/shard_map/all_to_all | solution.py:23
  88.1 0.0 copy-done.1
  88.1 1.7 shard_map.161
  89.8 27.9 %all_to_all.40 = bf16[32,4,256]{2,1,0:T(4,128)(2,1)S(1)} all-to-all(bf16[32,4,256]{2,1,0:T(4,128)(2,1)S(1)} %get-tuple-element.27), channel_id=1, replica_groups=mesh['grp'=2,'hi'=8,'mid'=2,'pair'=2,'tp'=8] {'hi','mid','pair'}, dimensions={0} | all-to-all | bytes 131072 | tf_op jit(solution)/shard_map/all_to_all | solution.py:23
  117.7 0.0 copy-done
  117.7 0.1 fusion
  117.9 0.7 broadcast_in_dim.30
  118.6 7.9 %all-to-all-start.3 = ((bf16[8,64,128]{2,1,0:T(8,128)(2,1)}), bf16[8,64,128]{2,1,0:T(8,128)(2,1)S(1)}, u32[]{:S(2)}, u32[]{:S(2)}) async-start(bf16[8,64,128]{2,1,0:T(8,128)(2,1)} %broadcast_in_dim.30), calls=%async_computation.3 | async-start | bytes 262144 | tf_op jit(solution)/shard_map/all_to_all | solution.py:23
  126.5 1.9 collective-permute-start.1
  128.4 2.4 %collective-permute-start.2 = (bf16[128,256]{1,0:T(8,128)(2,1)S(1)}, bf16[128,256]{1,0:T(8,128)(2,1)S(1)}, u32[]{:S(2)}, u32[]{:S(2)}) collective-permute-start(bf16[128,256]{1,0:T(8,128)(2,1)S(1)} %get-tuple-element.32), channel_id=1, source_target_pairs={{0,16},{8,24},{16,0},{24,8},{1,17},{9,25},{17,1},{25,9},{2,18},{10... | collective-permute-start | bytes 196616 | tf_op jit(solution)/shard_map/ppermute | solution.py:238
  130.8 5.0 %collective-permute-start.3 = (bf16[128,256]{1,0:T(8,128)(2,1)S(1)}, bf16[128,256]{1,0:T(8,128)(2,1)S(1)}, u32[]{:S(2)}, u32[]{:S(2)}) collective-permute-start(bf16[128,256]{1,0:T(8,128)(2,1)S(1)} %get-tuple-element.33), channel_id=1, source_target_pairs={{0,24},{8,16},{16,8},{24,0},{1,25},{9,17},{17,9},{25,1},{2,26},{10... | collective-permute-start | bytes 196616 | tf_op jit(solution)/shard_map/ppermute | solution.py:238
  135.8 0.0 all-to-all-done.3.arrived
  135.9 0.0 collective-permute-done.1.refs_1_
  135.9 0.0 collective-permute-done.2.refs_2_
  135.9 1.8 collective-permute-done.3.refs_3_
  137.7 8.7 %all_to_all.41.middle = bf16[4,64,128]{2,1,0:T(8,128)(2,1)S(1)} all-to-all(bf16[4,64,128]{2,1,0:T(8,128)(2,1)S(1)} %get-tuple-element.34), channel_id=1, replica_groups=mesh['grp'=2,'hi'=8,'mid'=2,'pair'=2,'tp'=8] {'mid','pair'}, dimensions={0} | all-to-all | bytes 131072 | tf_op jit(solution)/shard_map/all_to_all | solution.py:23
  146.4 0.3 shard_map.163
  146.7 24.1 %all_to_all.42 = bf16[8,40,128]{2,1,0:T(8,128)(2,1)S(1)} all-to-all(bf16[8,40,128]{2,1,0:T(8,128)(2,1)S(1)} %shard_map.163), channel_id=1, replica_groups=mesh['grp'=2,'hi'=8,'mid'=2,'pair'=2,'tp'=8] {'hi'}, dimensions={0} | all-to-all | bytes 163840 | tf_op jit(solution)/shard_map/all_to_all | solution.py:23
  170.9 26.1 %all_to_all.43.hidden = bf16[8,32,128]{2,1,0:T(8,128)(2,1)S(1)} all-to-all(bf16[8,32,128]{2,1,0:T(8,128)(2,1)S(1)} %broadcast_in_dim.31), channel_id=1, replica_groups=mesh['grp'=2,'hi'=8,'mid'=2,'pair'=2,'tp'=8] {'hi'}, dimensions={0} | all-to-all | bytes 131072 | tf_op jit(solution)/shard_map/all_to_all | solution.py:23
  196.9 0.8 shard_map.164
  197.8 11.8 %all-to-all-start.7 = ((bf16[32,8,128]{2,1,0:T(8,128)(2,1)}), bf16[32,8,128]{2,1,0:T(8,128)(2,1)S(1)}, u32[]{:S(2)}, u32[]{:S(2)}) async-start(bf16[32,8,128]{2,1,0:T(8,128)(2,1)} %shard_map.164), calls=%async_computation.7 | async-start | bytes 131072 | tf_op jit(solution)/shard_map/all_to_all | solution.py:23
  209.5 2.3 %shard_map.165 = f32[4,2,128,128]{3,2,1,0:T(8,128)} custom-call(f32[4,2,128,128]{3,2,1,0:T(8,128)} %state.3, f32[2,4,128]{2,1,0:T(4,128)S(1)} %get-tuple-element.39.keyed, f32[2,4,128]{2,1,0:T(4,128)S(1)} %get-tuple-element.40.fresh, f32[2,4,128]{2,1,0:T(4,128)S(1)} %get-tuple-element.41.decay), custom_call_target="tpu_custom_call" | custom-call | tf_op jit(solution)/shard_map/pallas_call | solution.py:195
  211.8 5.4 %all-to-all-done.7 = bf16[32,8,128]{2,1,0:T(8,128)(2,1)S(1)} async-done(((bf16[32,8,128]{2,1,0:T(8,128)(2,1)}), bf16[32,8,128]{2,1,0:T(8,128)(2,1)S(1)}, u32[]{:S(2)}, u32[]{:S(2)}) %all-to-all-start.7) | async-done | bytes 65568 | tf_op jit(solution)/shard_map/all_to_all | solution.py:23
  217.2 0.6 fusion.4
  (7 shorter events, 0.1 us)
Async XLA Ops:
  0.6 117.1 %copy-start = (bf16[256,64]{0,1:T(8,128)(2,1)S(1)}, bf16[256,64]{0,1:T(8,128)(2,1)}, u32[]{:S(2)}) copy-start(bf16[256,64]{0,1:T(8,128)(2,1)} %param.26) | copy-start | bytes 98308
  2.0 86.1 %copy-start.1 = (f32[4,2,128,128]{3,2,1,0:T(8,128)S(1)}, f32[4,2,128,128]{3,2,1,0:T(8,128)}, u32[]{:S(2)}) copy-start(f32[4,2,128,128]{3,2,1,0:T(8,128)} %state.3) | copy-start | bytes 1572868
  2.0 50.9 %all-to-all-start = ((bf16[16,8,128]{2,1,0:T(8,128)(2,1)}), bf16[16,8,128]{2,1,0:T(8,128)(2,1)S(1)}, u32[]{:S(2)}, u32[]{:S(2)}) async-start(bf16[16,8,128]{2,1,0:T(8,128)(2,1)} %broadcast_in_dim.24), calls=%async_computation | async-start | bytes 65536 | tf_op jit(solution)/shard_map/all_to_all | solution.py:23
  47.9 5.0 %collective-permute-start = (bf16[64,384]{1,0:T(8,128)(2,1)S(1)}, bf16[64,384]{1,0:T(8,128)(2,1)S(1)}, u32[]{:S(2)}, u32[]{:S(2)}) collective-permute-start(bf16[64,384]{1,0:T(8,128)(2,1)S(1)} %get-tuple-element.23), channel_id=1, source_target_pairs={{0,8},{8,0},{1,9},{9,1},{2,10},{10,2},{3,11},{11,3},{4,12},{12,4},... | collective-permute-start | bytes 147464 | tf_op jit(solution)/shard_map/ppermute | solution.py:349
  53.8 34.2 %all-to-all-start.1 = ((bf16[32,2,896]{2,1,0:T(2,128)(2,1)}), bf16[32,2,896]{2,1,0:T(2,128)(2,1)S(1)}, u32[]{:S(2)}, u32[]{:S(2)}) async-start(bf16[32,2,896]{2,1,0:T(2,128)(2,1)} %shard_map.159), calls=%async_computation.1 | async-start | bytes 229376 | tf_op jit(solution)/shard_map/all_to_all | solution.py:23
  118.6 17.3 %all-to-all-start.3 = ((bf16[8,64,128]{2,1,0:T(8,128)(2,1)}), bf16[8,64,128]{2,1,0:T(8,128)(2,1)S(1)}, u32[]{:S(2)}, u32[]{:S(2)}) async-start(bf16[8,64,128]{2,1,0:T(8,128)(2,1)} %broadcast_in_dim.30), calls=%async_computation.3 | async-start | bytes 262144 | tf_op jit(solution)/shard_map/all_to_all | solution.py:23
  126.5 9.4 %collective-permute-start.1 = (bf16[128,256]{1,0:T(8,128)(2,1)S(1)}, bf16[128,256]{1,0:T(8,128)(2,1)S(1)}, u32[]{:S(2)}, u32[]{:S(2)}) collective-permute-start(bf16[128,256]{1,0:T(8,128)(2,1)S(1)} %get-tuple-element.31), channel_id=1, source_target_pairs={{0,8},{8,0},{16,24},{24,16},{1,9},{9,1},{17,25},{25,17},{2,10},{10... | collective-permute-start | bytes 196616 | tf_op jit(solution)/shard_map/ppermute | solution.py:238
  128.4 7.5 %collective-permute-start.2 = (bf16[128,256]{1,0:T(8,128)(2,1)S(1)}, bf16[128,256]{1,0:T(8,128)(2,1)S(1)}, u32[]{:S(2)}, u32[]{:S(2)}) collective-permute-start(bf16[128,256]{1,0:T(8,128)(2,1)S(1)} %get-tuple-element.32), channel_id=1, source_target_pairs={{0,16},{8,24},{16,0},{24,8},{1,17},{9,25},{17,1},{25,9},{2,18},{10... | collective-permute-start | bytes 196616 | tf_op jit(solution)/shard_map/ppermute | solution.py:238
  130.8 6.9 %collective-permute-start.3 = (bf16[128,256]{1,0:T(8,128)(2,1)S(1)}, bf16[128,256]{1,0:T(8,128)(2,1)S(1)}, u32[]{:S(2)}, u32[]{:S(2)}) collective-permute-start(bf16[128,256]{1,0:T(8,128)(2,1)S(1)} %get-tuple-element.33), channel_id=1, source_target_pairs={{0,24},{8,16},{16,8},{24,0},{1,25},{9,17},{17,9},{25,1},{2,26},{10... | collective-permute-start | bytes 196616 | tf_op jit(solution)/shard_map/ppermute | solution.py:238
  197.8 19.4 %all-to-all-start.7 = ((bf16[32,8,128]{2,1,0:T(8,128)(2,1)}), bf16[32,8,128]{2,1,0:T(8,128)(2,1)S(1)}, u32[]{:S(2)}, u32[]{:S(2)}) async-start(bf16[32,8,128]{2,1,0:T(8,128)(2,1)} %shard_map.164), calls=%async_computation.7 | async-start | bytes 131072 | tf_op jit(solution)/shard_map/all_to_all | solution.py:23

commit v5 on v4

--- a/solution.py
+++ b/solution.py
@@ -156,17 +156,27 @@
     )(*sources)
 
 
-def sums_kernel(both, kept, taken, gates, sent):
-    n_kv, half, _ = sent.shape
-    side = lax.axis_index("pair")
-    mine = jnp.transpose(both[side].astype(f32))
-    other = jnp.transpose(both[1 - side].astype(f32))
+def own_kernel(both, kept, gates, main, tail):
+    mine = jnp.transpose(both[lax.axis_index("pair")].astype(f32))
     squares = jnp.sum(mine * mine, axis=1, keepdims=True)
     mine = mine.astype(bf16)
-    main = dotted(mine, kept[...], 1, 0) + dotted(other.astype(bf16), taken[...], 1, 0)
+    main[...] = dotted(mine, kept[...], 1, 0)
     extra = dotted(mine, gates[...], 1, 0)
     gap = jnp.zeros((mine.shape[0], TAIL - extra.shape[1] - 1), f32)
-    tail = jnp.concatenate([extra, squares, gap], axis=1)
+    tail[...] = jnp.concatenate([extra, squares, gap], axis=1)
+
+
+def own_sums(both, kept, gates):
+    rows = both.shape[2]
+    out = (pltpu.VMEM((rows, kept.shape[1]), f32), pltpu.VMEM((rows, TAIL), f32))
+    return pl.pallas_call(own_kernel, out_shape=out)(*in_vmem((both, kept, gates)))
+
+
+def sums_kernel(both, taken, own_main, own_tail, sent):
+    n_kv, half, _ = sent.shape
+    other = jnp.transpose(both[1 - lax.axis_index("pair")].astype(f32)).astype(bf16)
+    main = own_main[...] + dotted(other, taken[...], 1, 0)
+    tail = own_tail[...]
     blank = jnp.zeros_like(tail)
     upper = jnp.concatenate([main, tail, blank], axis=1)
     lower = jnp.concatenate([blank, tail], axis=1)
@@ -178,16 +188,11 @@
         sent[target] = jnp.concatenate([upper[top, :width], main[low], ends], axis=1).astype(bf16)
 
 
-def partial_sums(both, kept, taken, gates, n_kv, seq):
-    whole = pl.BlockSpec(memory_space=pltpu.VMEM)
-    assert seq % 2 == 0 and gates.shape[1] < TAIL
-    columns = 2 * (kept.shape[1] + TAIL)
-    near = [pltpu.with_memory_space_constraint(x, pltpu.VMEM) for x in (both, kept, taken, gates)]
-    return pl.pallas_call(
-        sums_kernel,
-        in_specs=[whole] * 4,
-        out_shape=jax.ShapeDtypeStruct((n_kv, seq // 2, columns), bf16),
-    )(*near)
+def partial_sums(both, taken, main, tail, n_kv, seq):
+    assert seq % 2 == 0
+    shape = (n_kv, seq // 2, 2 * (main.shape[1] + TAIL))
+    near = in_vmem((both, taken, main, tail))
+    return pl.pallas_call(sums_kernel, out_shape=jax.ShapeDtypeStruct(shape, bf16))(*near)
 
 
 def state_update(state, keyed, fresh, decay):
@@ -349,7 +354,8 @@
     taken = lax.ppermute(given, "pair", [(0, 1), (1, 0)])
 
     both = from_everyone(tokens_t, ("pair", "tp")).reshape(2, block, rows)
-    sent = partial_sums(both, kept, taken, gates, n_kv, seq_here)
+    main, tail = own_sums(both, kept, gates)
+    sent = partial_sums(both, taken, main, tail, n_kv, seq_here)
     pieces = mixer_pieces(w_up, w_down, mixer_gain)
     arrived = exchange(sent, KV)
     arrived, pieces[0] = lax.optimization_barrier((arrived, pieces[0]))

time: 219 us -> 218 us (level)
  no operation moved by 1% of the time
where the time goes in v5:
time: 218 us
  blocking collectives  86.8 us (40%)
  starting transfers between devices  84.7 us (39%)
  waiting for transfers between devices  34.1 us (16%)
  Pallas kernels  8.4 us (4%)
    all_to_all x4, blocking collectives, exchange(): return lax.all_to_all(x, axis, split_axis=0, concat_axis=0, tiled=True)  86.8 us
    all_to_all x4, starting transfers between devices, exchange(): return lax.all_to_all(x, axis, split_axis=0, concat_axis=0, tiled=True)  71.9 us
    all_to_all x4, waiting for transfers between devices, exchange(): return lax.all_to_all(x, axis, split_axis=0, concat_axis=0, tiled=True)  32.3 us
    ppermute x3, starting transfers between devices, mixer_pieces(): piece = lax.ppermute(piece, LO, [(i, i ^ step) for i in range(near)])  9.35 us
  transfers between devices with their start and end apart: 8, of which 4 were waited for; matrix products, arithmetic and copies ran while one was open for 0% of the time, Pallas kernels for 2%

profile of v5, /device:TPU:33, one launch (start us, length us, event | category | flops | bytes accessed | tf_op | source)
XLA Modules:
  0.0 217.5 jit_solution(17939440233358401898)
XLA Ops:
  0.6 0.0 copy-start
  0.6 1.3 broadcast_in_dim.24
  2.0 44.7 %all-to-all-start = ((bf16[16,8,128]{2,1,0:T(8,128)(2,1)}), bf16[16,8,128]{2,1,0:T(8,128)(2,1)S(1)}, u32[]{:S(2)}, u32[]{:S(2)}) async-start(bf16[16,8,128]{2,1,0:T(8,128)(2,1)} %broadcast_in_dim.24), calls=%async_computation | async-start | bytes 65536 | tf_op jit(solution)/shard_map/all_to_all | solution.py:23
  46.7 1.0 shard_map.158
  47.7 3.4 %collective-permute-start = (bf16[64,384]{1,0:T(8,128)(2,1)S(1)}, bf16[64,384]{1,0:T(8,128)(2,1)S(1)}, u32[]{:S(2)}, u32[]{:S(2)}) collective-permute-start(bf16[64,384]{1,0:T(8,128)(2,1)S(1)} %get-tuple-element.24), channel_id=1, source_target_pairs={{0,8},{8,0},{1,9},{9,1},{2,10},{10,2},{3,11},{11,3},{4,12},{12,4},... | collective-permute-start | bytes 147464 | tf_op jit(solution)/shard_map/ppermute | solution.py:354
  51.2 1.5 all-to-all-done
  52.7 0.0 copy-start.1
  52.7 0.3 shard_map.159
  53.0 0.0 collective-permute-done.taken
  53.0 0.9 shard_map.160
  53.9 7.5 %all-to-all-start.1 = ((bf16[32,2,896]{2,1,0:T(2,128)(2,1)}), bf16[32,2,896]{2,1,0:T(2,128)(2,1)S(1)}, u32[]{:S(2)}, u32[]{:S(2)}) async-start(bf16[32,2,896]{2,1,0:T(2,128)(2,1)} %shard_map.160), calls=%async_computation.1 | async-start | bytes 229376 | tf_op jit(solution)/shard_map/all_to_all | solution.py:23
  61.4 1.1 shard_map.161
  62.5 25.4 %all-to-all-done.1.arrived = bf16[32,2,896]{2,1,0:T(2,128)(2,1)S(1)} async-done(((bf16[32,2,896]{2,1,0:T(2,128)(2,1)}), bf16[32,2,896]{2,1,0:T(2,128)(2,1)S(1)}, u32[]{:S(2)}, u32[]{:S(2)}) %all-to-all-start.1) | async-done | bytes 114720 | tf_op jit(solution)/shard_map/all_to_all | solution.py:23
  87.9 0.0 copy-done.1
  87.9 1.7 shard_map.162
  89.5 27.9 %all_to_all.40 = bf16[32,4,256]{2,1,0:T(4,128)(2,1)S(1)} all-to-all(bf16[32,4,256]{2,1,0:T(4,128)(2,1)S(1)} %get-tuple-element.31), channel_id=1, replica_groups=mesh['grp'=2,'hi'=8,'mid'=2,'pair'=2,'tp'=8] {'hi','mid','pair'}, dimensions={0} | all-to-all | bytes 131072 | tf_op jit(solution)/shard_map/all_to_all | solution.py:23
  117.5 0.0 copy-done
  117.5 0.1 fusion
  117.6 0.7 broadcast_in_dim.30
  118.3 7.9 %all-to-all-start.3 = ((bf16[8,64,128]{2,1,0:T(8,128)(2,1)}), bf16[8,64,128]{2,1,0:T(8,128)(2,1)S(1)}, u32[]{:S(2)}, u32[]{:S(2)}) async-start(bf16[8,64,128]{2,1,0:T(8,128)(2,1)} %broadcast_in_dim.30), calls=%async_computation.3 | async-start | bytes 262144 | tf_op jit(solution)/shard_map/all_to_all | solution.py:23
  126.2 1.9 collective-permute-start.1
  128.1 2.4 %collective-permute-start.2 = (bf16[128,256]{1,0:T(8,128)(2,1)S(1)}, bf16[128,256]{1,0:T(8,128)(2,1)S(1)}, u32[]{:S(2)}, u32[]{:S(2)}) collective-permute-start(bf16[128,256]{1,0:T(8,128)(2,1)S(1)} %get-tuple-element.36), channel_id=1, source_target_pairs={{0,16},{8,24},{16,0},{24,8},{1,17},{9,25},{17,1},{25,9},{2,18},{10... | collective-permute-start | bytes 196616 | tf_op jit(solution)/shard_map/ppermute | solution.py:243
  130.5 5.0 %collective-permute-start.3 = (bf16[128,256]{1,0:T(8,128)(2,1)S(1)}, bf16[128,256]{1,0:T(8,128)(2,1)S(1)}, u32[]{:S(2)}, u32[]{:S(2)}) collective-permute-start(bf16[128,256]{1,0:T(8,128)(2,1)S(1)} %get-tuple-element.37), channel_id=1, source_target_pairs={{0,24},{8,16},{16,8},{24,0},{1,25},{9,17},{17,9},{25,1},{2,26},{10... | collective-permute-start | bytes 196616 | tf_op jit(solution)/shard_map/ppermute | solution.py:243
  135.6 0.0 all-to-all-done.3.arrived
  135.6 0.0 collective-permute-done.1.refs_1_
  135.6 0.0 collective-permute-done.2.refs_2_
  135.6 1.8 collective-permute-done.3.refs_3_
  137.5 8.7 %all_to_all.41.middle = bf16[4,64,128]{2,1,0:T(8,128)(2,1)S(1)} all-to-all(bf16[4,64,128]{2,1,0:T(8,128)(2,1)S(1)} %get-tuple-element.38), channel_id=1, replica_groups=mesh['grp'=2,'hi'=8,'mid'=2,'pair'=2,'tp'=8] {'mid','pair'}, dimensions={0} | all-to-all | bytes 131072 | tf_op jit(solution)/shard_map/all_to_all | solution.py:23
  146.1 0.3 shard_map.164
  146.4 24.1 %all_to_all.42 = bf16[8,40,128]{2,1,0:T(8,128)(2,1)S(1)} all-to-all(bf16[8,40,128]{2,1,0:T(8,128)(2,1)S(1)} %shard_map.164), channel_id=1, replica_groups=mesh['grp'=2,'hi'=8,'mid'=2,'pair'=2,'tp'=8] {'hi'}, dimensions={0} | all-to-all | bytes 163840 | tf_op jit(solution)/shard_map/all_to_all | solution.py:23
  170.6 26.1 %all_to_all.43.hidden = bf16[8,32,128]{2,1,0:T(8,128)(2,1)S(1)} all-to-all(bf16[8,32,128]{2,1,0:T(8,128)(2,1)S(1)} %broadcast_in_dim.31), channel_id=1, replica_groups=mesh['grp'=2,'hi'=8,'mid'=2,'pair'=2,'tp'=8] {'hi'}, dimensions={0} | all-to-all | bytes 131072 | tf_op jit(solution)/shard_map/all_to_all | solution.py:23
  196.7 0.8 shard_map.165
  197.5 11.8 %all-to-all-start.7 = ((bf16[32,8,128]{2,1,0:T(8,128)(2,1)}), bf16[32,8,128]{2,1,0:T(8,128)(2,1)S(1)}, u32[]{:S(2)}, u32[]{:S(2)}) async-start(bf16[32,8,128]{2,1,0:T(8,128)(2,1)} %shard_map.165), calls=%async_computation.7 | async-start | bytes 131072 | tf_op jit(solution)/shard_map/all_to_all | solution.py:23
  209.3 2.3 %shard_map.166 = f32[4,2,128,128]{3,2,1,0:T(8,128)} custom-call(f32[4,2,128,128]{3,2,1,0:T(8,128)} %state.3, f32[2,4,128]{2,1,0:T(4,128)S(1)} %get-tuple-element.43.keyed, f32[2,4,128]{2,1,0:T(4,128)S(1)} %get-tuple-element.44.fresh, f32[2,4,128]{2,1,0:T(4,128)S(1)} %get-tuple-element.45.decay), custom_call_target="tpu_custom_call" | custom-call | tf_op jit(solution)/shard_map/pallas_call | solution.py:200
  211.6 5.4 %all-to-all-done.7 = bf16[32,8,128]{2,1,0:T(8,128)(2,1)S(1)} async-done(((bf16[32,8,128]{2,1,0:T(8,128)(2,1)}), bf16[32,8,128]{2,1,0:T(8,128)(2,1)S(1)}, u32[]{:S(2)}, u32[]{:S(2)}) %all-to-all-start.7) | async-done | bytes 65568 | tf_op jit(solution)/shard_map/all_to_all | solution.py:23
  217.0 0.6 fusion.4
  (7 shorter events, 0.1 us)
Async XLA Ops:
  0.6 116.8 %copy-start = (bf16[256,64]{0,1:T(8,128)(2,1)S(1)}, bf16[256,64]{0,1:T(8,128)(2,1)}, u32[]{:S(2)}) copy-start(bf16[256,64]{0,1:T(8,128)(2,1)} %param.26) | copy-start | bytes 98308
  2.0 50.7 %all-to-all-start = ((bf16[16,8,128]{2,1,0:T(8,128)(2,1)}), bf16[16,8,128]{2,1,0:T(8,128)(2,1)S(1)}, u32[]{:S(2)}, u32[]{:S(2)}) async-start(bf16[16,8,128]{2,1,0:T(8,128)(2,1)} %broadcast_in_dim.24), calls=%async_computation | async-start | bytes 65536 | tf_op jit(solution)/shard_map/all_to_all | solution.py:23
  47.7 5.2 %collective-permute-start = (bf16[64,384]{1,0:T(8,128)(2,1)S(1)}, bf16[64,384]{1,0:T(8,128)(2,1)S(1)}, u32[]{:S(2)}, u32[]{:S(2)}) collective-permute-start(bf16[64,384]{1,0:T(8,128)(2,1)S(1)} %get-tuple-element.24), channel_id=1, source_target_pairs={{0,8},{8,0},{1,9},{9,1},{2,10},{10,2},{3,11},{11,3},{4,12},{12,4},... | collective-permute-start | bytes 147464 | tf_op jit(solution)/shard_map/ppermute | solution.py:354
  52.7 35.2 %copy-start.1 = (f32[4,2,128,128]{3,2,1,0:T(8,128)S(1)}, f32[4,2,128,128]{3,2,1,0:T(8,128)}, u32[]{:S(2)}) copy-start(f32[4,2,128,128]{3,2,1,0:T(8,128)} %state.3) | copy-start | bytes 1572868
  53.9 34.0 %all-to-all-start.1 = ((bf16[32,2,896]{2,1,0:T(2,128)(2,1)}), bf16[32,2,896]{2,1,0:T(2,128)(2,1)S(1)}, u32[]{:S(2)}, u32[]{:S(2)}) async-start(bf16[32,2,896]{2,1,0:T(2,128)(2,1)} %shard_map.160), calls=%async_computation.1 | async-start | bytes 229376 | tf_op jit(solution)/shard_map/all_to_all | solution.py:23
  118.3 17.3 %all-to-all-start.3 = ((bf16[8,64,128]{2,1,0:T(8,128)(2,1)}), bf16[8,64,128]{2,1,0:T(8,128)(2,1)S(1)}, u32[]{:S(2)}, u32[]{:S(2)}) async-start(bf16[8,64,128]{2,1,0:T(8,128)(2,1)} %broadcast_in_dim.30), calls=%async_computation.3 | async-start | bytes 262144 | tf_op jit(solution)/shard_map/all_to_all | solution.py:23
  126.2 9.4 %collective-permute-start.1 = (bf16[128,256]{1,0:T(8,128)(2,1)S(1)}, bf16[128,256]{1,0:T(8,128)(2,1)S(1)}, u32[]{:S(2)}, u32[]{:S(2)}) collective-permute-start(bf16[128,256]{1,0:T(8,128)(2,1)S(1)} %get-tuple-element.35), channel_id=1, source_target_pairs={{0,8},{8,0},{16,24},{24,16},{1,9},{9,1},{17,25},{25,17},{2,10},{10... | collective-permute-start | bytes 196616 | tf_op jit(solution)/shard_map/ppermute | solution.py:243
  128.1 7.5 %collective-permute-start.2 = (bf16[128,256]{1,0:T(8,128)(2,1)S(1)}, bf16[128,256]{1,0:T(8,128)(2,1)S(1)}, u32[]{:S(2)}, u32[]{:S(2)}) collective-permute-start(bf16[128,256]{1,0:T(8,128)(2,1)S(1)} %get-tuple-element.36), channel_id=1, source_target_pairs={{0,16},{8,24},{16,0},{24,8},{1,17},{9,25},{17,1},{25,9},{2,18},{10... | collective-permute-start | bytes 196616 | tf_op jit(solution)/shard_map/ppermute | solution.py:243
  130.5 6.9 %collective-permute-start.3 = (bf16[128,256]{1,0:T(8,128)(2,1)S(1)}, bf16[128,256]{1,0:T(8,128)(2,1)S(1)}, u32[]{:S(2)}, u32[]{:S(2)}) collective-permute-start(bf16[128,256]{1,0:T(8,128)(2,1)S(1)} %get-tuple-element.37), channel_id=1, source_target_pairs={{0,24},{8,16},{16,8},{24,0},{1,25},{9,17},{17,9},{25,1},{2,26},{10... | collective-permute-start | bytes 196616 | tf_op jit(solution)/shard_map/ppermute | solution.py:243
  197.5 19.4 %all-to-all-start.7 = ((bf16[32,8,128]{2,1,0:T(8,128)(2,1)}), bf16[32,8,128]{2,1,0:T(8,128)(2,1)S(1)}, u32[]{:S(2)}, u32[]{:S(2)}) async-start(bf16[32,8,128]{2,1,0:T(8,128)(2,1)} %shard_map.165), calls=%async_computation.7 | async-start | bytes 131072 | tf_op jit(solution)/shard_map/all_to_all | solution.py:23
